TPU v7x, 32 devices: a whole 2x2x4 slice. The times are simulated.
32 devices in a mesh: sp: 8 (over z, x), tp: 4 (over y, core).
Axes of the slice: x: 2, y: 2, z: 4, core: 2. Of those that a mesh axis runs over, the one named last changes fastest.
Arguments:
- queries: bfloat16 [2048, 1024], P('sp', 'tp'), may hold values from -6 to 6
- keys: bfloat16 [2048, 256], P('sp'), may hold values from -6 to 6
- values: bfloat16 [2048, 256], P('sp'), may hold values from -6 to 6
- sink: float32 [16], P('tp'), may hold values from 3 to 6
- w_out: bfloat16 [1024, 2048], P('tp'), may hold values from -0.1875 to 0.1875
- stream: bfloat16 [2048, 2048], P(('sp', 'tp')), may hold values from -6 to 6
- gain: bfloat16 [2048], replicated, may hold values from 0.099609375 to 1.8984375
- routes: int32 [2048, 4], P('sp'), may hold values from 0 to 63, all different within a row; in each aligned block of 64 rows (0 to 63, 64 to 127, ...) at most 8 rows name the same one
- route_weights: float32 [2048, 4], P('sp'), may hold values from 0.2 to 1
- w_gate: bfloat16 [64, 1024, 2048], P('sp', 'tp'), may hold values from -0.125 to 0.125
- w_up: bfloat16 [64, 1024, 2048], P('sp', 'tp'), may hold values from -0.125 to 0.125
- w_down: bfloat16 [64, 1024, 2048], P('sp', None, 'tp'), may hold values from -0.1875 to 0.1875
- shared_gate: bfloat16 [1024, 2048], P('tp'), may hold values from -0.125 to 0.125
- shared_up: bfloat16 [1024, 2048], P('tp'), may hold values from -0.125 to 0.125
- shared_down: bfloat16 [1024, 2048], P(None, 'tp'), may hold values from -0.1875 to 0.1875
Outputs:
- layer_out: bfloat16 [2048, 2048], P('sp', 'tp')
Inputs may be any that keep to these rules, and one draw needn't show every extreme that they name: `routes`: in each aligned block of 64 rows no expert is named in more than 8 rows, and some blocks reach 8; a row names 4 different experts.
All inputs are finite; a program needn't handle non-finite values.
Results may differ from a plain program's by a relative error of at most 0.014.
Values may be sent and summed in bfloat16 or wider, within the bound.
No kernel may reach another device: no remote copies, remote signals or barrier semaphores. Data moves between devices by JAX's collectives and lax.ppermute only.
A program may use at most 128 MiB of HBM per device.

v0:
```python
import jax
import jax.numpy as jnp
from jax import lax
from jax.sharding import PartitionSpec as P

D = 2048
HEADS = 16
KV_HEADS = 4
HD = 64
WINDOW = 128
EXPERTS = 64
TOPK = 4


NORM_EPS = 1e-05


def with_halo(array, sides, width):
    for axis, dim in sides:
        devices, length = (lax.axis_size(axis), array.shape[dim])
        up = [(i, (i + 1) % devices) for i in range(devices - 1)]
        down = [(j, i) for i, j in up]
        last = lax.slice_in_dim(array, length - width, length, axis=dim)
        leading = lax.slice_in_dim(array, 0, width, axis=dim)
        before = lax.ppermute(last, axis, up)
        after = lax.ppermute(leading, axis, down)
        array = jnp.concatenate([before, array, after], axis=dim)
    return array


def slot_ids(block_routes, capacity):
    flat_routes = block_routes.reshape(-1)
    hit_table = (flat_routes[:, None] == jnp.arange(EXPERTS)[None, :]).astype(jnp.int32)
    earlier = jnp.cumsum(hit_table, axis=0) - hit_table
    slot_rank = jnp.sum(earlier * hit_table, axis=1)
    return flat_routes * capacity + slot_rank


def local(
    queries,
    keys,
    values,
    sink,
    w_out,
    stream,
    gain,
    routes,
    route_weights,
    w_gate,
    w_up,
    w_down,
    shared_gate,
    shared_up,
    shared_down,
):
    tok_dev = queries.shape[0]
    n_tp = lax.axis_size("tp")
    n_sp = lax.axis_size("sp")
    tp_idx = lax.axis_index("tp")
    sp_idx = lax.axis_index("sp")
    heads_dev = HEADS // n_tp
    group = HEADS // KV_HEADS
    kv_head = tp_idx * heads_dev // group
    key_own = lax.dynamic_slice_in_dim(keys, kv_head * HD, HD, 1)
    value_own = lax.dynamic_slice_in_dim(values, kv_head * HD, HD, 1)
    paired = jnp.concatenate([key_own, value_own], axis=1)
    padded = with_halo(paired, (("sp", 0),), WINDOW)
    blocks = tok_dev // WINDOW
    framed = padded.reshape(blocks + 2, WINDOW, 2 * HD)
    banded = jnp.concatenate([framed[:-2], framed[1:-1], framed[2:]], axis=1)
    key_band = banded[:, :, :HD]
    value_band = banded[:, :, HD:]
    query_blocks = queries.reshape(blocks, WINDOW, heads_dev, HD)
    scores = jnp.einsum(
        "nqhd,njd->nhqj", query_blocks, key_band, preferred_element_type=jnp.float32
    ) * HD ** (-0.5)
    offset = sp_idx * tok_dev
    seq_total = tok_dev * n_sp
    query_pos = (
        offset + jnp.arange(blocks)[:, None, None] * WINDOW + jnp.arange(WINDOW)[None, :, None]
    )
    key_pos = (
        offset
        - WINDOW
        + jnp.arange(blocks)[:, None, None] * WINDOW
        + jnp.arange(3 * WINDOW)[None, None, :]
    )
    allowed = (jnp.abs(query_pos - key_pos) <= WINDOW) & (key_pos >= 0) & (key_pos < seq_total)
    scores = jnp.where(allowed[:, None], scores, -jnp.inf)
    sink_level = sink.reshape(1, heads_dev, 1, 1)
    row_peak = jnp.maximum(scores.max(-1, keepdims=True), sink_level)
    probabilities = jnp.exp(scores - row_peak)
    denominator = probabilities.sum(-1, keepdims=True) + jnp.exp(sink_level - row_peak)
    weights = (probabilities / denominator).astype(jnp.bfloat16)
    attended = jnp.einsum("nhqj,njd->nqhd", weights, value_band, preferred_element_type=jnp.float32)
    attended = attended.astype(jnp.bfloat16).reshape(tok_dev, heads_dev * HD)
    rows_dev = tok_dev // n_tp
    d_dev = w_down.shape[2]
    projected = lax.psum_scatter(
        jnp.dot(attended, w_out, preferred_element_type=jnp.float32),
        "tp",
        scatter_dimension=0,
        tiled=True,
    )
    mixed_rows = (stream.astype(jnp.float32) + projected).astype(jnp.bfloat16)
    whole_rows = lax.all_gather(mixed_rows, "tp", axis=0, tiled=True)
    wide_rows = whole_rows.astype(jnp.float32)
    scale_rows = lax.rsqrt(jnp.mean(wide_rows * wide_rows, axis=-1, keepdims=True) + NORM_EPS)
    normed = (wide_rows * scale_rows * gain.astype(jnp.float32)).astype(jnp.bfloat16)
    residual = lax.dynamic_slice_in_dim(wide_rows, tp_idx * d_dev, d_dev, 1)
    exp_dev = w_gate.shape[0]
    capacity = max(1, 2 * tok_dev * TOPK // (n_tp * EXPERTS))
    slot_count = EXPERTS * capacity
    blocked_routes = routes.reshape(n_tp, rows_dev, TOPK)
    destination = jax.vmap(lambda block_routes: slot_ids(block_routes, capacity))(blocked_routes)
    slot_select = destination[:, None, :] == jnp.arange(slot_count)[None, :, None]
    slot_select = slot_select.reshape(n_tp, slot_count, rows_dev, TOPK).astype(jnp.float32)
    dispatch_table = jnp.sum(slot_select, axis=-1).astype(jnp.bfloat16)
    combine_table = jnp.sum(slot_select * route_weights.reshape(n_tp, 1, rows_dev, TOPK), axis=-1)
    normed_blocks = normed.reshape(n_tp, rows_dev, D)
    own_table = lax.dynamic_index_in_dim(dispatch_table, tp_idx, 0, keepdims=False)
    own_rows = lax.dynamic_index_in_dim(normed_blocks, tp_idx, 0, keepdims=False)
    outgoing = jnp.dot(own_table, own_rows, preferred_element_type=jnp.float32).astype(jnp.bfloat16)
    arrived = lax.all_to_all(outgoing, "sp", split_axis=0, concat_axis=0, tiled=True)
    arrived = arrived.reshape(1, n_sp, exp_dev, capacity, D)
    piece_rows = lax.all_gather(arrived, "tp", axis=0, tiled=True)
    gate_act = jnp.einsum(
        "tsecd,efd->tsecf", piece_rows, w_gate, preferred_element_type=jnp.float32
    )
    up_act = jnp.einsum("tsecd,efd->tsecf", piece_rows, w_up, preferred_element_type=jnp.float32)
    hidden = (jax.nn.silu(gate_act) * up_act).astype(jnp.bfloat16)
    shared_gate_act = jnp.einsum(
        "td,fd->tf", normed, shared_gate, preferred_element_type=jnp.float32
    )
    shared_up_act = jnp.einsum("td,fd->tf", normed, shared_up, preferred_element_type=jnp.float32)
    shared_hidden = (jax.nn.silu(shared_gate_act) * shared_up_act).astype(jnp.bfloat16)
    shared_hidden = shared_hidden.reshape(1, 1, 1, tok_dev, shared_hidden.shape[1])
    expert_piece = lax.all_gather(hidden, "tp", axis=4, tiled=True)
    shared_piece = lax.all_gather(shared_hidden, "tp", axis=4, tiled=True)
    piece_width = expert_piece.shape[4]
    routed_total = jnp.einsum(
        "tsecf,efd->tsecd", expert_piece, w_down, preferred_element_type=jnp.float32
    )
    shared_total = jnp.dot(
        shared_piece.reshape(tok_dev, piece_width), shared_down, preferred_element_type=jnp.float32
    )
    returned = lax.all_to_all(
        routed_total.astype(jnp.bfloat16), "sp", split_axis=1, concat_axis=1, tiled=True
    )
    returned = returned.reshape(n_tp, slot_count, d_dev).astype(jnp.float32)
    routed = jnp.einsum("tmr,tmd->trd", combine_table, returned, precision=lax.Precision.HIGHEST)
    routed = routed.reshape(tok_dev, d_dev)
    return (residual + routed + shared_total).astype(jnp.bfloat16)


def solution(mesh):
    placed = (
        P("sp", "tp"),
        P("sp", None),
        P("sp", None),
        P("tp"),
        P("tp", None),
        P(("sp", "tp"), None),
        P(),
        P("sp", None),
        P("sp", None),
        P("sp", "tp", None),
        P("sp", "tp", None),
        P("sp", None, "tp"),
        P("tp", None),
        P("tp", None),
        P(None, "tp"),
    )
    return jax.shard_map(
        local, mesh=mesh, in_specs=placed, out_specs=P("sp", "tp"), check_vma=False
    )
```

profile of v0, /device:TPU:0, one launch (start us, length us, event | category | flops | bytes accessed | tf_op | source)
XLA Modules:
  0.0 317.8 jit_solution(6857469026317906916)
XLA Ops:
  6.5 1.1 constant_dynamic-slice_fusion
  7.6 0.1 fusion.32
  7.7 4.9 %collective-permute-start = (bf16[128,128]{1,0:T(8,128)(2,1)S(1)}, bf16[128,128]{1,0:T(8,128)(2,1)S(1)}, u32[]{:S(2)}, u32[]{:S(2)}) collective-permute-start(bf16[128,128]{1,0:T(8,128)(2,1)S(1)} %get-tuple-element.10), channel_id=1, source_target_pairs={{0,4},{4,8},{8,12},{12,16},{16,20},{20,24},{24,28},{1,5},{5,9},{9,... | collective-permute-start | bytes 98312 | tf_op jit(solution)/shard_map/ppermute | solution.py:25
  12.6 1.3 collective-permute-start.1
  13.9 0.1 iota_add_fusion
  14.0 0.1 fusion.37
  14.1 0.1 iota_add_fusion.1
  14.2 0.5 fusion.19
  14.6 1.1 reshape.199
  15.7 2.7 collective-permute-done.1
  18.4 0.1 pad_maximum_fusion.3
  18.5 0.1 copy.55
  18.6 0.1 copy.54
  18.8 0.1 copy.53
  18.9 0.4 fusion.41
  19.4 0.1 broadcast_maximum_fusion
  19.5 0.2 fusion.14
  19.7 0.1 exponential_add_fusion
  19.8 0.4 fusion.17
  20.2 0.1 copy.59
  20.4 1.8 fusion.27
  22.2 0.0 reduce-scatter.2.cloned.1.call-update
  22.2 0.0 all-gather.5.cloned.1.call-start
  22.3 32.5 %reduce-scatter.2.cloned.1.call-done = f32[64,2048]{1,0:T(8,128)} async-done(((f32[256,2048]{1,0:T(8,128)}), f32[64,2048]{1,0:T(8,128)}) %reduce-scatter.2.cloned.1.call-update) | async-done | bytes 524304 | tf_op jit(solution)/shard_map/reduce_scatter | solution.py:99
  54.7 1.8 add_convert_fusion
  56.5 0.0 all-gather.5.cloned.1.call-update
  56.5 0.0 all-gather.7.cloned.1.call-start
  56.6 0.1 copy.61
  56.7 0.1 eq.39
  56.9 0.1 eq.43
  57.0 0.1 copy.60
  57.2 2.4 reduce-window.6
  59.6 0.1 slice.53
  59.7 0.1 copy.63
  59.9 0.2 fusion.22
  60.0 0.1 reduce_sum.49
  60.2 0.1 copy.66
  60.3 0.1 mul.107
  60.4 1.3 convert_reduce_fusion
  61.7 11.7 %all-gather.5.cloned.1.call-done = bf16[256,2048]{1,0:T(8,128)(2,1)} async-done(((bf16[64,2048]{1,0:T(8,128)(2,1)}), bf16[256,2048]{1,0:T(8,128)(2,1)}) %all-gather.5.cloned.1.call-update) | async-done | bytes 1048592 | tf_op jit(solution)/shard_map/all_gather | solution.py:106
  73.4 1.5 multiply_reduce_fusion
  74.9 1.5 multiply_convert_fusion
  76.5 0.7 convolution_convert_fusion
  77.2 53.9 %all_to_all.14 = bf16[8,64,2048]{2,1,0:T(8,128)(2,1)S(1)} all-to-all(bf16[8,64,2048]{2,1,0:T(8,128)(2,1)S(1)} %bitcast.114), channel_id=1, replica_groups=mesh['sp'=8,'tp'=4] {'sp'}, dimensions={0} | all-to-all | bytes 4194304 | tf_op jit(solution)/shard_map/all_to_all | solution.py:124
  131.1 1.5 copy.68
  132.6 0.2 all-gather.9.cloned.1.call-start
  132.8 56.3 %all-gather.7.cloned.1.call-done = bf16[4,8,8,8,2048]{4,3,1,0,2:T(8,128)(2,1)} async-done(((bf16[1,8,8,8,2048]{4,3,1,0,2:T(8,128)(2,1)}), bf16[4,8,8,8,2048]{4,3,1,0,2:T(8,128)(2,1)}) %all-gather.7.cloned.1.call-update) | async-done | bytes 8388624 | tf_op jit(solution)/shard_map/all_gather | solution.py:126
  189.2 8.1 %fusion.4 = f32[8,4,8,8,256]{4,3,2,1,0:T(8,128)S(1)} fusion(bf16[4,8,8,8,2048]{4,3,1,0,2:T(8,128)(2,1)} %all-gather.7.cloned.1.call-done, bf16[8,256,2048]{2,1,0:T(8,128)(2,1)} %param.24), kind=kOutput, calls=%fused_computation.4 | convolution fusion | flops 2147483648 | bytes 18874368 | tf_op jit(solution)/shard_map/tsecd,efd->tsecf/dot_general | solution.py:127
  197.3 11.4 %fusion.6 = bf16[4,8,8,8,256]{4,3,1,0,2:T(8,128)(2,1)} fusion(f32[8,4,8,8,256]{4,3,2,1,0:T(8,128)S(1)} %fusion.4, bf16[4,8,8,8,2048]{4,3,1,0,2:T(8,128)(2,1)} %all-gather.7.cloned.1.call-done, bf16[8,256,2048]{2,1,0:T(8,128)(2,1)} %param.25), kind=kOutput, calls=%fused_computation.8 | convolution fusion | flops 2150629376 | bytes 19922944 | tf_op jit(solution)/shard_map/tsecd,efd->tsecf/dot_general | solution.py:130
  208.7 35.2 %all-gather.9.cloned.1.call-done = bf16[4,8,8,8,1024]{4,3,1,0,2:T(8,128)(2,1)} async-done(((bf16[4,8,8,8,256]{4,3,1,0,2:T(8,128)(2,1)}), bf16[4,8,8,8,1024]{4,3,1,0,2:T(8,128)(2,1)}) %all-gather.9.cloned.1.call-update) | async-done | bytes 4194320 | tf_op jit(solution)/shard_map/all_gather | solution.py:138
  243.8 7.0 %convert_bitcast_fusion = bf16[4,8,8,8,512]{4,3,1,0,2:T(8,128)(2,1)S(1)} fusion(bf16[4,8,8,8,1024]{4,3,1,0,2:T(8,128)(2,1)} %all-gather.9.cloned.1.call-done, bf16[8,1024,512]{2,1,0:T(8,128)(2,1)} %param.26), kind=kOutput, calls=%fused_computation.14 | convolution fusion | flops 2148532224 | bytes 14680064 | tf_op jit(solution)/shard_map/tsecf,efd->tsecd/dot_general | solution.py:141
  250.8 1.6 copy.69
  252.4 5.6 %all-to-all-start.1 = ((bf16[4,8,8,8,512]{4,3,0,2,1:T(8,128)(2,1)}), bf16[4,8,8,8,512]{4,3,0,2,1:T(8,128)(2,1)S(1)}, u32[]{:S(2)}, u32[]{:S(2)}) async-start(bf16[4,8,8,8,512]{4,3,0,2,1:T(8,128)(2,1)} %copy.69), calls=%async_computation.2 | async-start | bytes 4194304 | tf_op jit(solution)/shard_map/all_to_all | solution.py:147
  258.1 1.6 convert_element_type.61
  259.7 0.7 copy-done.7
  260.4 0.5 fusion.43
  260.8 0.5 fusion.16
  261.3 7.4 %all-gather = bf16[256,1024]{1,0:T(8,128)(2,1)} all-gather(bf16[256,256]{1,0:T(8,128)(2,1)S(1)} %fusion.16), channel_id=2, replica_groups=mesh['sp'=8,'tp'=4] {'tp'}, dimensions={1}, use_global_device_ids=true | all-gather | bytes 655360 | tf_op jit(solution)/shard_map/all_gather | solution.py:139
  268.7 38.0 %all-to-all-done.1 = bf16[4,8,8,8,512]{4,3,0,2,1:T(8,128)(2,1)S(1)} async-done(((bf16[4,8,8,8,512]{4,3,0,2,1:T(8,128)(2,1)}), bf16[4,8,8,8,512]{4,3,0,2,1:T(8,128)(2,1)S(1)}, u32[]{:S(2)}, u32[]{:S(2)}) %all-to-all-start.1) | async-done | bytes 2097184 | tf_op jit(solution)/shard_map/all_to_all | solution.py:147
  306.7 0.3 copy.70
  307.0 0.8 copy-done.6
  307.8 1.2 fusion.42
  308.9 1.1 bitcast_add_fusion
  310.1 1.1 fusion.15
  (44 shorter events, 0.2 us)
Async XLA Ops:
  6.5 13.8 %copy-start = (bf16[256,2048]{1,0:T(8,128)(2,1)S(1)}, bf16[256,2048]{1,0:T(8,128)(2,1)}, u32[]{:S(2)}) copy-start(bf16[256,2048]{1,0:T(8,128)(2,1)} %param.19) | copy-start | bytes 3145732
  6.5 48.2 %reduce-scatter.2.cloned.1.call-start = ((), (), s32[]{:S(2)}) async-start(), calls=%async_computation.3 | async-start | bytes 2621440 | tf_op jit(solution)/shard_map/reduce_scatter | solution.py:99
  6.5 12.9 %copy-start.13 = (f32[4]{0:T(128)S(1)}, f32[4]{0:T(128)}, u32[]{:S(2)}) copy-start(f32[4]{0:T(128)} %param.18) | copy-start | bytes 52
  7.7 8.0 %collective-permute-start = (bf16[128,128]{1,0:T(8,128)(2,1)S(1)}, bf16[128,128]{1,0:T(8,128)(2,1)S(1)}, u32[]{:S(2)}, u32[]{:S(2)}) collective-permute-start(bf16[128,128]{1,0:T(8,128)(2,1)S(1)} %get-tuple-element.10), channel_id=1, source_target_pairs={{0,4},{4,8},{8,12},{12,16},{16,20},{20,24},{24,28},{1,5},{5,9},{9,... | collective-permute-start | bytes 98312 | tf_op jit(solution)/shard_map/ppermute | solution.py:25
  12.6 5.8 %collective-permute-start.1 = (bf16[128,128]{1,0:T(8,128)(2,1)S(1)}, bf16[128,128]{1,0:T(8,128)(2,1)S(1)}, u32[]{:S(2)}, u32[]{:S(2)}) collective-permute-start(bf16[128,128]{1,0:T(8,128)(2,1)S(1)} %get-tuple-element.11), channel_id=1, source_target_pairs={{4,0},{8,4},{12,8},{16,12},{20,16},{24,20},{28,24},{5,1},{9,5},{13... | collective-permute-start | bytes 98312 | tf_op jit(solution)/shard_map/ppermute | solution.py:26
  20.4 34.4 %copy-start.9 = (bf16[64,2048]{1,0:T(8,128)(2,1)S(1)}, bf16[64,2048]{1,0:T(8,128)(2,1)}, u32[]{:S(2)}) copy-start(bf16[64,2048]{1,0:T(8,128)(2,1)} %param.20) | copy-start | bytes 786436
  22.2 34.4 %copy-start.10 = (s32[256,4]{0,1:T(4,128)S(1)}, s32[256,4]{0,1:T(4,128)}, u32[]{:S(2)}) copy-start(s32[256,4]{0,1:T(4,128)} %param.22) | copy-start | bytes 12292
  22.2 38.1 %copy-start.11 = (f32[256,4]{0,1:T(4,128)S(1)}, f32[256,4]{0,1:T(4,128)}, u32[]{:S(2)}) copy-start(f32[256,4]{0,1:T(4,128)} %param.23) | copy-start | bytes 12292
  22.2 38.2 %copy-start.12 = (bf16[2048]{0:T(1024)(128)(2,1)S(1)}, bf16[2048]{0:T(1024)(128)(2,1)}, u32[]{:S(2)}) copy-start(bf16[2048]{0:T(1024)(128)(2,1)} %param.21) | copy-start | bytes 12292
  22.2 51.2 %all-gather.5.cloned.1.call-start = ((), (), s32[]{:S(2)}) async-start(), calls=%async_computation.4 | async-start | bytes 1310720 | tf_op jit(solution)/shard_map/all_gather | solution.py:106
  56.5 132.6 %all-gather.7.cloned.1.call-start = ((), (), s32[]{:S(2)}) async-start(), calls=%async_computation.5 | async-start | bytes 10485760 | tf_op jit(solution)/shard_map/all_gather | solution.py:126
  76.5 54.6 %copy-start.3 = (bf16[256,2048]{1,0:T(8,128)(2,1)}, bf16[256,2048]{1,0:T(8,128)(2,1)S(1)}, u32[]{:S(2)}) copy-start(bf16[256,2048]{1,0:T(8,128)(2,1)S(1)} %multiply_convert_fusion) | copy-start | bytes 3145732
  132.6 111.2 %all-gather.9.cloned.1.call-start = ((), (), s32[]{:S(2)}) async-start(), calls=%async_computation.6 | async-start | bytes 5242880 | tf_op jit(solution)/shard_map/all_gather | solution.py:138
  252.4 5.6 %copy-start.2 = (bf16[256,2048]{1,0:T(8,128)(2,1)S(1)}, bf16[256,2048]{1,0:T(8,128)(2,1)}, u32[]{:S(2)}) copy-start(bf16[256,2048]{1,0:T(8,128)(2,1)} %all-gather.5.cloned.1.call-done) | copy-start | bytes 3145732
  252.4 54.3 %all-to-all-start.1 = ((bf16[4,8,8,8,512]{4,3,0,2,1:T(8,128)(2,1)}), bf16[4,8,8,8,512]{4,3,0,2,1:T(8,128)(2,1)S(1)}, u32[]{:S(2)}, u32[]{:S(2)}) async-start(bf16[4,8,8,8,512]{4,3,0,2,1:T(8,128)(2,1)} %copy.69), calls=%async_computation.2 | async-start | bytes 4194304 | tf_op jit(solution)/shard_map/all_to_all | solution.py:147
  258.1 1.6 copy-start.4
  258.1 2.3 copy-start.7
  258.1 2.8 copy-start.14
  306.7 1.0 copy-start.6
  307.8 2.3 copy-start.5
  307.8 2.3 copy-start.8
  307.8 3.5 %copy-start.1 = (bf16[256,2048]{1,0:T(8,128)(2,1)S(1)}, bf16[256,2048]{1,0:T(8,128)(2,1)}, u32[]{:S(2)}) copy-start(bf16[256,2048]{1,0:T(8,128)(2,1)} %param.19) | copy-start | bytes 3145732
Sparse Core Ops, SparseCore 0:
  22.3 32.3 reduce-scatter.1
  56.7 16.6 all-gather.4
  132.7 56.3 all-gather.6
  208.8 34.9 all-gather.8
where the time goes:
time: 318 us
  waiting for transfers between devices  176 us (55%)
  blocking collectives  61.2 us (19%)
  matrix products  33.1 us (10%)
  between operations  13.5 us (4%)
  other arithmetic  12.7 us (4%)
  starting transfers between devices  12.1 us (4%)
  local copies, waits for them, and re-layouts  8.65 us (3%)
    all_gather x1, waiting for transfers between devices, local(): piece_rows = lax.all_gather(arrived, 'tp', axis=0, tiled=True)  56.3 us
    all_to_all x1, blocking collectives, local(): lax.all_to_all(outgoing, 'sp', split_axis=0, concat_axis=0, tiled=True)  53.9 us
    all_to_all x1, waiting for transfers between devices, local(): lax.all_to_all(routed_total.astype(jnp.bfloat16), 'sp', split_axis=1, con...  38 us
    all_gather x1, waiting for transfers between devices, local(): expert_piece = lax.all_gather(hidden, 'tp', axis=4, tiled=True)  35.2 us
    reduce_scatter x1, waiting for transfers between devices, local(): lax.psum_scatter(jnp.dot(attended, w_out, preferred_element_type=jnp.floa...  32.5 us
    all_gather x1, waiting for transfers between devices, local(): whole_rows = lax.all_gather(mixed_rows, 'tp', axis=0, tiled=True)  11.7 us
    dot_general x1, matrix products, local(): jnp.einsum('tsecd,efd->tsecf', piece_rows, w_up, preferred_element_type=j...  11.4 us
    dot_general x1, matrix products, local(): jnp.einsum('tsecd,efd->tsecf', piece_rows, w_gate, preferred_element_type...  8.13 us
  transfers between devices with their start and end apart: 7, of which 6 were waited for; matrix products, arithmetic and copies ran while one was open for 3% of the time, Pallas kernels for 0%

commit v1 on v0

--- a/solution.py
+++ b/solution.py
@@ -1,7 +1,12 @@
+import functools
+
 import jax
 import jax.numpy as jnp
 from jax import lax
+from jax.experimental import pallas as pl
+from jax.experimental.pallas import tpu as pltpu
 from jax.sharding import PartitionSpec as P
+
 
 D = 2048
 HEADS = 16
@@ -13,6 +18,11 @@
 
 
 NORM_EPS = 1e-05
+LANES = 128
+AHEAD = 2
+DOWN_AHEAD = 4
+UP_VMEM = 36 * 1024 * 1024
+DOWN_VMEM = 20 * 1024 * 1024
 
 
 def with_halo(array, sides, width):
@@ -36,23 +46,7 @@
     return flat_routes * capacity + slot_rank
 
 
-def local(
-    queries,
-    keys,
-    values,
-    sink,
-    w_out,
-    stream,
-    gain,
-    routes,
-    route_weights,
-    w_gate,
-    w_up,
-    w_down,
-    shared_gate,
-    shared_up,
-    shared_down,
-):
+def attention(queries, keys, values, sink):
     tok_dev = queries.shape[0]
     n_tp = lax.axis_size("tp")
     n_sp = lax.axis_size("sp")
@@ -93,7 +87,31 @@
     denominator = probabilities.sum(-1, keepdims=True) + jnp.exp(sink_level - row_peak)
     weights = (probabilities / denominator).astype(jnp.bfloat16)
     attended = jnp.einsum("nhqj,njd->nqhd", weights, value_band, preferred_element_type=jnp.float32)
-    attended = attended.astype(jnp.bfloat16).reshape(tok_dev, heads_dev * HD)
+    return attended.astype(jnp.bfloat16).reshape(tok_dev, heads_dev * HD)
+
+
+def local_general(
+    queries,
+    keys,
+    values,
+    sink,
+    w_out,
+    stream,
+    gain,
+    routes,
+    route_weights,
+    w_gate,
+    w_up,
+    w_down,
+    shared_gate,
+    shared_up,
+    shared_down,
+):
+    tok_dev = queries.shape[0]
+    n_tp = lax.axis_size("tp")
+    n_sp = lax.axis_size("sp")
+    tp_idx = lax.axis_index("tp")
+    attended = attention(queries, keys, values, sink)
     rows_dev = tok_dev // n_tp
     d_dev = w_down.shape[2]
     projected = lax.psum_scatter(
@@ -153,6 +171,369 @@
     return (residual + routed + shared_total).astype(jnp.bfloat16)
 
 
+def in_vmem(a):
+    return pltpu.with_memory_space_constraint(a, pltpu.MemorySpace.VMEM)
+
+
+NT = (((1,), (1,)), ((), ()))
+
+
+def silu_product(gate, up):
+    return (gate / (1.0 + jnp.exp(-gate)) * up).astype(jnp.bfloat16)
+
+
+def spots(rows, shape, where_ref, axis):
+    quad = lax.broadcasted_iota(jnp.int32, shape, axis) // rows
+    return jnp.bitwise_xor(quad, where_ref[1])
+
+
+def up_kernel(where_ref, *refs, places, count, own, exp_dev, capacity, quads, rows):
+    pieces_hbm = refs[:count]
+    gate_hbm, up_hbm = refs[count : count + 2]
+    rest = refs[count + 2 :]
+    pieces, piece_sems = rest[-2:]
+    rest = rest[:-2]
+    piece_copies = [
+        pltpu.make_async_copy(ref, pieces.at[i], piece_sems.at[i])
+        for i, ref in enumerate(pieces_hbm)
+    ]
+    for copy in piece_copies:
+        copy.start()
+    shared_copies = []
+    if own:
+        shared_hbm, rest = rest[:2], rest[2:]
+        sgate_ref, sup_ref, shared_sems = rest[-3:]
+        rest = rest[:-3]
+        for i, ref in enumerate((sgate_ref, sup_ref)):
+            shared_copies.append(pltpu.make_async_copy(shared_hbm[i], ref, shared_sems.at[i]))
+            shared_copies[-1].start()
+    hidden_ref, table_ref = rest[:2]
+    weights_ref, slots_ref, sems = rest[-3:]
+    piece = gate_hbm.shape[1]
+    copies = []
+    for e in range(exp_dev):
+        copies.append(
+            (
+                pltpu.make_async_copy(gate_hbm.at[e], weights_ref.at[e, :piece], sems.at[0, e]),
+                pltpu.make_async_copy(up_hbm.at[e], weights_ref.at[e, piece:], sems.at[1, e]),
+            )
+        )
+    for e in range(min(AHEAD, exp_dev)):
+        for copy in copies[e]:
+            copy.start()
+
+    width = quads * capacity
+    lanes = exp_dev * width
+    tokens = quads * rows
+
+    def slot(shape, axis):
+        index = lax.broadcasted_iota(jnp.int32, shape, axis)
+        return index // width, (index // capacity) % quads, index % capacity
+
+    column = lax.broadcasted_iota(jnp.int32, (lanes, 2 * EXPERTS), 1)
+    expert = slot((lanes, 2 * EXPERTS), 0)[0] + where_ref[0]
+    of_rank = (column == expert).astype(jnp.float32).astype(jnp.bfloat16)
+    of_weight = (column == expert + EXPERTS).astype(jnp.float32).astype(jnp.bfloat16)
+
+    def wanted(axis):
+        shape = (lanes, tokens) if axis == 0 else (tokens, lanes)
+        _, spot, rank = slot(shape, axis)
+        same = spot == spots(rows, shape, where_ref, 1 - axis)
+        return jnp.where(same, rank + 1, -1).astype(jnp.float32)
+
+    by_slot, by_token = wanted(0), wanted(1)
+    for unit, members in enumerate(places):
+        for ref in members:
+            piece_copies[ref].wait()
+        extra = jnp.concatenate([pieces[ref, :, D:] for ref in members], axis=0)
+        held = jnp.concatenate([pieces[ref, :, :D] for ref in members], axis=0)
+        ranks = lax.dot_general(of_rank, extra, NT, preferred_element_type=jnp.float32)
+        table = jnp.where(ranks == by_slot, 1.0, 0.0).astype(jnp.bfloat16)
+        picked = jnp.dot(table, held, preferred_element_type=jnp.float32).astype(jnp.bfloat16)
+        for e in range(exp_dev):
+            slots_ref[e, unit * width : (unit + 1) * width, :] = picked[e * width : (e + 1) * width]
+        ranks = lax.dot_general(extra, of_rank, NT, preferred_element_type=jnp.float32)
+        weights = lax.dot_general(extra, of_weight, NT, preferred_element_type=jnp.float32)
+        table = jnp.where(ranks == by_token, weights, 0.0).astype(jnp.bfloat16)
+        for quad in range(quads):
+            start = pl.multiple_of(jnp.bitwise_xor(where_ref[1], quad) * rows, rows)
+            table_ref[unit, pl.ds(start, rows), :] = table[quad * rows : (quad + 1) * rows]
+        if own and unit == 0:
+            for copy in shared_copies:
+                copy.wait()
+            gate = lax.dot_general(held, sgate_ref[...], NT, preferred_element_type=jnp.float32)
+            up = lax.dot_general(held, sup_ref[...], NT, preferred_element_type=jnp.float32)
+            hidden = silu_product(gate, up)
+            for quad in range(quads):
+                start = jnp.bitwise_xor(where_ref[1], quad) * rows
+                tall = hidden_ref.shape[1]
+                hidden_ref[
+                    exp_dev + start // tall, pl.ds(pl.multiple_of(start % tall, rows), rows), :
+                ] = hidden[quad * rows : (quad + 1) * rows]
+    for e in range(exp_dev):
+        for copy in copies[e]:
+            copy.wait()
+        if e + AHEAD < exp_dev:
+            for copy in copies[e + AHEAD]:
+                copy.start()
+        held = slots_ref[e]
+        both = lax.dot_general(held, weights_ref[e], NT, preferred_element_type=jnp.float32)
+        hidden_ref[e] = silu_product(both[:, :piece], both[:, piece:])
+
+
+def down_kernel(where_ref, *refs, own, units, quads, exp_dev, capacity, piece):
+    hiddens = refs[:quads]
+    table_ref, down_hbm = refs[quads : quads + 2]
+    rest = refs[quads + 2 :]
+    if own:
+        sdown_hbm, shared_ref = rest[:2]
+        sdown_ref, shared_sem = rest[-2:]
+        rest = rest[2:]
+        shared_copy = pltpu.make_async_copy(sdown_hbm, sdown_ref, shared_sem)
+        shared_copy.start()
+    outs = rest[:units]
+    downs, result_ref, sems = rest[units:][:3]
+    copies = [
+        pltpu.make_async_copy(down_hbm.at[e], downs.at[e], sems.at[e]) for e in range(exp_dev)
+    ]
+    for copy in copies[:DOWN_AHEAD]:
+        copy.start()
+    width = quads * capacity
+
+    def product(parts, weight_ref, lead):
+        total = None
+        for quad, part in enumerate(parts):
+            start = pl.multiple_of(jnp.bitwise_xor(where_ref[1], quad) * piece, piece)
+            weight = weight_ref[lead + (pl.ds(start, piece), slice(None))]
+            term = jnp.dot(part, weight, preferred_element_type=jnp.float32)
+            total = term if total is None else total + term
+        return total
+
+    if own:
+        shared_copy.wait()
+        tall = hiddens[0].shape[1]
+        for part in range(shared_ref.shape[0] // tall):
+            shared_ref[part * tall : (part + 1) * tall] = product(
+                [ref[exp_dev + part] for ref in hiddens], sdown_ref, ()
+            )
+    for e in range(exp_dev):
+        copies[e].wait()
+        if e + DOWN_AHEAD < exp_dev:
+            copies[e + DOWN_AHEAD].start()
+        total = product([ref[e] for ref in hiddens], downs, (e,)).astype(jnp.bfloat16)
+        for unit in range(units):
+            result_ref[unit, e * width : (e + 1) * width, :] = total[
+                unit * width : (unit + 1) * width
+            ]
+    for unit in range(units):
+        routed = jnp.dot(table_ref[unit], result_ref[unit], preferred_element_type=jnp.float32)
+        outs[unit][...] = routed.astype(jnp.bfloat16)
+
+
+def local_torus(
+    queries,
+    keys,
+    values,
+    sink,
+    w_out,
+    stream,
+    gain,
+    routes,
+    route_weights,
+    w_gate,
+    w_up,
+    w_down,
+    shared_gate,
+    shared_up,
+    shared_down,
+    *,
+    nx,
+):
+    tok_dev = queries.shape[0]
+    n_tp = lax.axis_size("tp")
+    n_sp = lax.axis_size("sp")
+    nz = n_sp // nx
+    tp_idx = lax.axis_index("tp")
+    sp_idx = lax.axis_index("sp")
+    rows = tok_dev // n_tp
+    d_dev = w_down.shape[2]
+    exp_dev = w_gate.shape[0]
+    piece = w_gate.shape[1]
+    capacity = max(1, 2 * tok_dev * TOPK // (n_tp * EXPERTS))
+    bf16, f32 = jnp.bfloat16, jnp.float32
+
+    def swap(a, axis, bit):
+        pairs = [(i, i ^ bit) for i in range(lax.axis_size(axis))]
+        return lax.ppermute(a, axis, pairs)
+
+    def core_swap(a):
+        return swap(a, "tp", 1)
+
+    def y_swap(a):
+        return swap(a, "tp", 2)
+
+    def x_swap(a):
+        return swap(a, "sp", 1)
+
+    def z_swap(a, bit):
+        return swap(a, "sp", bit * nx)
+
+    own_routes = lax.dynamic_slice_in_dim(routes, tp_idx * rows, rows, 0)
+    own_weights = lax.dynamic_slice_in_dim(route_weights, tp_idx * rows, rows, 0)
+    hits = own_routes[:, :, None] == jnp.arange(EXPERTS)[None, None, :]
+    named = jnp.any(hits, axis=1)
+    not_later = (jnp.arange(rows)[:, None] >= jnp.arange(rows)[None, :]).astype(bf16)
+    ranks = jnp.dot(not_later, named.astype(bf16), preferred_element_type=f32)
+    extra = jnp.concatenate(
+        [
+            jnp.where(named, ranks, 0.0),
+            jnp.sum(jnp.where(hits, own_weights[:, :, None], 0.0), axis=1),
+        ],
+        axis=1,
+    ).astype(bf16)
+
+    attended = attention(queries, keys, values, sink)
+    projected = jnp.dot(attended, w_out, preferred_element_type=f32)
+    quarters = projected.reshape(n_tp // 2, 2, rows, D)
+    core = tp_idx % 2
+    own_y = tp_idx // 2
+    keep = lax.dynamic_index_in_dim(quarters, core, 1, keepdims=False)
+    give = lax.dynamic_index_in_dim(quarters, 1 - core, 1, keepdims=False)
+    chip = keep + core_swap(give.astype(bf16)).astype(f32)
+    away = lax.dynamic_index_in_dim(chip, 1 - own_y, 0, keepdims=False).astype(bf16)
+    home = lax.dynamic_index_in_dim(chip, own_y, 0, keepdims=False)
+    summed = home + y_swap(away).astype(f32)
+    mixed = (stream.astype(f32) + summed).astype(bf16)
+    wide = mixed.astype(f32)
+    scale = lax.rsqrt(jnp.mean(wide * wide, axis=-1, keepdims=True) + NORM_EPS)
+    normed = (wide * scale * gain.astype(f32)).astype(bf16)
+    own = jnp.concatenate([normed, extra], axis=1)
+
+    chunk_z = nz // 2
+    far = [own, z_swap(own, 1), z_swap(own, 2)]
+    far.append(z_swap(far[2], 1))
+    chunks = [([], []), ([], [])]
+    for k in range(nz):
+        operands, places = chunks[1 - k // chunk_z]
+        by_x, by_y = x_swap(far[k]), y_swap(far[k])
+        both = y_swap(by_x) if k in (1, 2) else x_swap(by_y)
+        base = len(operands)
+        for rows_in in (far[k], by_y, by_x, both):
+            operands += [rows_in, core_swap(rows_in)]
+        places += [range(base, base + n_tp), range(base + n_tp, base + 2 * n_tp)]
+    quads = n_tp
+
+    def columns(a, index, width):
+        return lax.dynamic_slice_in_dim(a, index * width, width, 1)
+
+    half = 2 * d_dev
+    near_y = columns(mixed, own_y, half)
+    far_y = y_swap(columns(mixed, 1 - own_y, half))
+    by_y = jnp.concatenate([near_y, far_y], axis=0)
+    here = columns(by_y, core, d_dev)
+    there = core_swap(columns(by_y, 1 - core, d_dev))
+    both = jnp.stack([here[:rows], there[:rows], here[rows:], there[rows:]], axis=0)
+    residual = jnp.take(both, jnp.arange(n_tp) ^ tp_idx, axis=0).reshape(tok_dev, d_dev)
+
+    where = jnp.stack([sp_idx * exp_dev, tp_idx]).astype(jnp.int32)
+    width = quads * capacity
+    lanes = exp_dev * width
+    smem = pl.BlockSpec(memory_space=pltpu.SMEM)
+    vmem = pl.BlockSpec(memory_space=pltpu.VMEM)
+    hbm = pl.BlockSpec(memory_space=pltpu.MemorySpace.HBM)
+
+    def in_hbm(*arrays):
+        return [pltpu.with_memory_space_constraint(a, pltpu.MemorySpace.HBM) for a in arrays]
+
+    def up_call(operands, places, own):
+        units = len(places)
+        shared = [shared_gate, shared_up] if own else []
+        kernel = functools.partial(
+            up_kernel,
+            places=places,
+            count=len(operands),
+            own=own,
+            exp_dev=exp_dev,
+            capacity=capacity,
+            quads=quads,
+            rows=rows,
+        )
+        groups = exp_dev + (tok_dev // (units * width) if own else 0)
+        out_shape = [
+            jax.ShapeDtypeStruct((groups, units * width, piece), bf16),
+            jax.ShapeDtypeStruct((units, tok_dev, lanes), bf16),
+        ]
+        return pl.pallas_call(
+            kernel,
+            in_specs=[smem] + [hbm] * (len(operands) + 2 + len(shared)),
+            out_specs=[vmem] * len(out_shape),
+            out_shape=out_shape,
+            scratch_shapes=[
+                pltpu.VMEM((exp_dev, 2 * piece, D), bf16),
+                pltpu.VMEM((exp_dev, units * width, D), bf16),
+                pltpu.SemaphoreType.DMA((2, exp_dev)),
+            ]
+            + [pltpu.VMEM((piece, D), bf16)] * len(shared)
+            + [pltpu.SemaphoreType.DMA((2,))] * (len(shared) // 2)
+            + [
+                pltpu.VMEM((len(operands), rows, D + LANES), bf16),
+                pltpu.SemaphoreType.DMA((len(operands),)),
+            ],
+            compiler_params=pltpu.CompilerParams(vmem_limit_bytes=UP_VMEM),
+            name="up_kernel",
+        )(where, *in_hbm(*operands, w_gate, w_up, *shared))
+
+    def down_call(hiddens, table, own):
+        units = table.shape[0]
+        kernel = functools.partial(
+            down_kernel,
+            own=own,
+            units=units,
+            quads=quads,
+            exp_dev=exp_dev,
+            capacity=capacity,
+            piece=piece,
+        )
+        out_shape = [jax.ShapeDtypeStruct((tok_dev, d_dev), bf16)] * units
+        more = []
+        if own:
+            out_shape = [jax.ShapeDtypeStruct((tok_dev, d_dev), f32)] + out_shape
+            more = [shared_down]
+        return pl.pallas_call(
+            kernel,
+            in_specs=[smem] + [vmem] * (quads + 1) + [hbm] * (1 + len(more)),
+            out_specs=[vmem] * len(out_shape),
+            out_shape=out_shape,
+            scratch_shapes=[
+                pltpu.VMEM((exp_dev, quads * piece, d_dev), bf16),
+                pltpu.VMEM((units, lanes, d_dev), bf16),
+                pltpu.SemaphoreType.DMA((exp_dev,)),
+            ]
+            + [pltpu.VMEM((quads * piece, d_dev), bf16), pltpu.SemaphoreType.DMA] * len(more),
+            compiler_params=pltpu.CompilerParams(vmem_limit_bytes=DOWN_VMEM),
+            name="down_kernel",
+        )(where, *map(in_vmem, hiddens), table, *in_hbm(w_down, *more))
+
+    total = residual.astype(f32)
+    sums = {}
+    for chunk, (operands, places) in enumerate(chunks):
+        hidden, table = up_call(operands, places, chunk == 1)
+        by_y = y_swap(hidden)
+        hiddens = [hidden, core_swap(hidden)]
+        hiddens += [by_y, core_swap(by_y)]
+        parts = list(down_call(hiddens, table, chunk == 1))
+        if chunk == 1:
+            total += parts.pop(0)
+        for pair in range(chunk_z):
+            k = (1 - chunk) * chunk_z + pair
+            there = x_swap(parts[pair * nx + 1])
+            sums[k] = parts[pair * nx].astype(f32) + there.astype(f32)
+    from_next = z_swap(sums[3].astype(bf16), 1)
+    from_far = z_swap((sums[2] + from_next.astype(f32)).astype(bf16), 2)
+    total += sums[0] + z_swap(sums[1].astype(bf16), 1).astype(f32)
+    return (total + from_far.astype(f32)).astype(bf16)
+
+
 def solution(mesh):
     placed = (
         P("sp", "tp"),
@@ -171,6 +552,22 @@
         P("tp", None),
         P(None, "tp"),
     )
+    n_sp, n_tp = mesh.shape["sp"], mesh.shape["tp"]
+    nx = 1
+    while 4 * nx * nx <= n_sp:
+        nx *= 2
+
+    pairs = nx == 2 and n_tp == 4 and n_sp == nx * 4
+
+    def local(*args):
+        tok_dev, piece = args[0].shape[0], args[9].shape[1]
+        capacity = 2 * tok_dev * TOPK // (n_tp * EXPERTS)
+        tiles = capacity % 8 == 0 and piece % LANES == 0 and (tok_dev // n_tp) % 16 == 0
+        slots = n_sp * n_tp * capacity == tok_dev
+        if pairs and tiles and slots:
+            return local_torus(*args, nx=nx)
+        return local_general(*args)
+
     return jax.shard_map(
         local, mesh=mesh, in_specs=placed, out_specs=P("sp", "tp"), check_vma=False
     )

time: 318 us -> 186 us (0.58)
  waiting for transfers between devices: 176 us -> 81.8 us
  blocking collectives: 61.2 us -> 0 us
  Pallas kernels: 0 us -> 40.4 us
  matrix products: 33.1 us -> 1.43 us
  starting transfers between devices: 12.1 us -> 39.2 us
  between operations: 13.5 us -> 0.77 us
  local copies, waits for them, and re-layouts: 8.65 us -> 13.5 us
  other arithmetic: 12.7 us -> 8.42 us
    all_gather x3 -> x0, waiting for transfers between devices: 103 us -> none  [the longest x1 56.3 us: local(): piece_rows = lax.all_gather(arrived, 'tp', axis=0, tiled=True)]
    ppermute x0 -> x48, waiting for transfers between devices: none -> 79.1 us  [swap(): return lax.ppermute(a, axis, pairs)]
    all_to_all x1 -> x0, blocking collectives: 53.9 us -> none  [local(): lax.all_to_all(outgoing, 'sp', split_axis=0, concat_axis=0, tiled=True)]
    pallas_call x0 -> x4, Pallas kernels: none -> 40.4 us  [the longest x2 26.3 us: up_call(): pl.pallas_call(kernel, in_specs=[smem] + [hbm] * (len(operands) + 2 + len...]
    all_to_all x1 -> x0, waiting for transfers between devices: 38 us -> none  [local(): lax.all_to_all(routed_total.astype(jnp.bfloat16), 'sp', split_axis=1, con...]
    ppermute x0 -> x48, starting transfers between devices: none -> 33 us  [swap(): return lax.ppermute(a, axis, pairs)]
    reduce_scatter x1 -> x0, waiting for transfers between devices: 32.5 us -> none  [local(): lax.psum_scatter(jnp.dot(attended, w_out, preferred_element_type=jnp.floa...]
    dot_general x11 -> x4, matrix products: 33.1 us -> 1.43 us  [the longest x1 0.46 us: local_torus(): projected = jnp.dot(attended, w_out, preferred_element_type=f32)]
  transfers between devices with their start and end apart: 7 -> 50, of which waited for: 6 -> 19; matrix products, arithmetic and copies ran while one was open for 3% -> 4% of each run, Pallas kernels for 0% -> 22%
where the time goes in v1:
time: 186 us; the launch traced here: 185 us
  waiting for transfers between devices  81.8 us (44%)
  Pallas kernels  40.4 us (22%)
  starting transfers between devices  39.2 us (21%)
  local copies, waits for them, and re-layouts  13.5 us (7%)
  other arithmetic  8.42 us (5%)
    ppermute x48, waiting for transfers between devices, swap(): return lax.ppermute(a, axis, pairs)  79.1 us
    ppermute x48, starting transfers between devices, swap(): return lax.ppermute(a, axis, pairs)  33 us
    pallas_call x2, Pallas kernels, up_call(): pl.pallas_call(kernel, in_specs=[smem] + [hbm] * (len(operands) + 2 + len...  26.3 us
    pallas_call x2, Pallas kernels, down_call(): pl.pallas_call(kernel, in_specs=[smem] + [vmem] * (quads + 1) + [hbm] * (...  14.1 us
    unnamed x80, local copies, waits for them, and re-layouts  6.07 us
    ppermute x1, starting transfers between devices, with_halo(): before = lax.ppermute(last, axis, up)  4.87 us
  transfers between devices with their start and end apart: 50, of which 19 were waited for; matrix products, arithmetic and copies ran while one was open for 4% of the time, Pallas kernels for 22%

profile of v1, /device:TPU:0, one launch (start us, length us, event | category | flops | bytes accessed | tf_op | source)
XLA Modules:
  0.0 185.5 jit_solution(8648004293679899820)
XLA Ops:
  0.0 1.1 constant_dynamic-slice_fusion.4
  1.2 4.9 %collective-permute-start = (bf16[128,128]{1,0:T(8,128)(2,1)S(1)}, bf16[128,128]{1,0:T(8,128)(2,1)S(1)}, u32[]{:S(2)}, u32[]{:S(2)}) collective-permute-start(bf16[128,128]{1,0:T(8,128)(2,1)S(1)} %get-tuple-element.44), channel_id=1, source_target_pairs={{0,4},{4,8},{8,12},{12,16},{16,20},{20,24},{24,28},{1,5},{5,9},{9,... | collective-permute-start | bytes 98312 | tf_op jit(solution)/shard_map/ppermute | solution.py:35
  6.1 1.3 collective-permute-start.1
  8.1 1.1 reshape.175
  9.2 2.6 %collective-permute-done.1 = bf16[128,128]{1,0:T(8,128)(2,1)S(1)} collective-permute-done((bf16[128,128]{1,0:T(8,128)(2,1)S(1)}, bf16[128,128]{1,0:T(8,128)(2,1)S(1)}, u32[]{:S(2)}, u32[]{:S(2)}) %collective-permute-start.1) | collective-permute-done | bytes 32800 | tf_op jit(solution)/shard_map/ppermute | solution.py:36
  14.3 0.9 fusion.8
  15.5 1.9 %collective-permute-done.2 = bf16[2,64,2048]{2,1,0:T(8,128)(2,1)} collective-permute-done((bf16[2,64,2048]{2,1,0:T(8,128)(2,1)}, bf16[2,64,2048]{2,1,0:T(8,128)(2,1)}, u32[]{:S(2)}, u32[]{:S(2)}) %collective-permute-start.2) | collective-permute-done | bytes 524320 | tf_op jit(solution)/shard_map/ppermute | solution.py:367
  17.4 1.1 bitcast_add_fusion
  18.6 1.0 copy-done.11
  19.6 1.6 collective-permute-start.3
  21.4 6.6 %collective-permute-done.3 = bf16[64,2048]{1,0:T(8,128)(2,1)S(1)} collective-permute-done((bf16[64,2048]{1,0:T(8,128)(2,1)S(1)}, bf16[64,2048]{1,0:T(8,128)(2,1)S(1)}, u32[]{:S(2)}, u32[]{:S(2)}) %collective-permute-start.3) | collective-permute-done | bytes 262176 | tf_op jit(solution)/shard_map/ppermute | solution.py:367
  28.0 1.3 fusion.5
  29.3 0.7 copy-done.12
  30.2 2.6 %collective-permute-start.27 = (bf16[64,2176]{1,0:T(8,128)(2,1)S(1)}, bf16[64,2176]{1,0:T(8,128)(2,1)S(1)}, u32[]{:S(2)}, u32[]{:S(2)}) collective-permute-start(bf16[64,2176]{1,0:T(8,128)(2,1)S(1)} %concatenate.27.refs_0_), channel_id=1, source_target_pairs={{0,16},{4,20},{8,24},{12,28},{16,0},{20,4},{24,8},{28,12},{1,17},{... | collective-permute-start | bytes 835592 | tf_op jit(solution)/shard_map/ppermute | solution.py:367
  32.9 1.5 collective-permute-start.7
  34.4 2.5 %collective-permute-start.9 = (bf16[64,2176]{1,0:T(8,128)(2,1)S(1)}, bf16[64,2176]{1,0:T(8,128)(2,1)S(1)}, u32[]{:S(2)}, u32[]{:S(2)}) collective-permute-start(bf16[64,2176]{1,0:T(8,128)(2,1)S(1)} %concatenate.27.refs_0_), channel_id=1, source_target_pairs={{0,4},{4,0},{8,12},{12,8},{16,20},{20,16},{24,28},{28,24},{1,5},{5... | collective-permute-start | bytes 835592 | tf_op jit(solution)/shard_map/ppermute | solution.py:367
  36.8 8.2 %collective-permute-done.27.refs_0_ = bf16[64,2176]{1,0:T(8,128)(2,1)S(1)} collective-permute-done((bf16[64,2176]{1,0:T(8,128)(2,1)S(1)}, bf16[64,2176]{1,0:T(8,128)(2,1)S(1)}, u32[]{:S(2)}, u32[]{:S(2)}) %collective-permute-start.27) | collective-permute-done | bytes 278560 | tf_op jit(solution)/shard_map/ppermute | solution.py:367
  45.1 1.6 collective-permute-start.29
  46.7 2.5 %collective-permute-start.31 = (bf16[64,2176]{1,0:T(8,128)(2,1)S(1)}, bf16[64,2176]{1,0:T(8,128)(2,1)S(1)}, u32[]{:S(2)}, u32[]{:S(2)}) collective-permute-start(bf16[64,2176]{1,0:T(8,128)(2,1)S(1)} %collective-permute-done.27.refs_0_), channel_id=1, source_target_pairs={{0,4},{4,0},{8,12},{12,8},{16,20},{20,16},{24,28},{28,24},{1,5},{5... | collective-permute-start | bytes 835592 | tf_op jit(solution)/shard_map/ppermute | solution.py:367
  49.2 1.0 collective-permute-done.13.refs_8_
  50.2 0.5 collective-permute-start.10
  50.7 3.5 %collective-permute-done.29.refs_2_ = bf16[64,2176]{1,0:T(8,128)(2,1)S(1)} collective-permute-done((bf16[64,2176]{1,0:T(8,128)(2,1)S(1)}, bf16[64,2176]{1,0:T(8,128)(2,1)S(1)}, u32[]{:S(2)}, u32[]{:S(2)}) %collective-permute-start.29) | collective-permute-done | bytes 278560 | tf_op jit(solution)/shard_map/ppermute | solution.py:367
  54.2 2.4 %collective-permute-start.11 = (bf16[64,2176]{1,0:T(8,128)(2,1)S(1)}, bf16[64,2176]{1,0:T(8,128)(2,1)}, u32[]{:S(2)}, u32[]{:S(2)}) collective-permute-start(bf16[64,2176]{1,0:T(8,128)(2,1)S(1)} %collective-permute-done.7.refs_2_), channel_id=1, source_target_pairs={{0,4},{4,0},{8,12},{12,8},{16,20},{20,16},{24,28},{28,24},{1,5},{5... | collective-permute-start | bytes 835592 | tf_op jit(solution)/shard_map/ppermute | solution.py:367
  56.6 1.5 collective-permute-start.15
  58.4 1.6 collective-permute-start.37
  60.0 4.2 %collective-permute-done.11.refs_6_ = bf16[64,2176]{1,0:T(8,128)(2,1)} collective-permute-done((bf16[64,2176]{1,0:T(8,128)(2,1)S(1)}, bf16[64,2176]{1,0:T(8,128)(2,1)}, u32[]{:S(2)}, u32[]{:S(2)}) %collective-permute-start.11) | collective-permute-done | bytes 278560 | tf_op jit(solution)/shard_map/ppermute | solution.py:367
  64.2 2.0 %collective-permute-done.15.refs_10_ = bf16[64,2176]{1,0:T(8,128)(2,1)} collective-permute-done((bf16[64,2176]{1,0:T(8,128)(2,1)S(1)}, bf16[64,2176]{1,0:T(8,128)(2,1)}, u32[]{:S(2)}, u32[]{:S(2)}) %collective-permute-start.15) | collective-permute-done | bytes 278560 | tf_op jit(solution)/shard_map/ppermute | solution.py:367
  66.3 1.5 collective-permute-start.33
  67.8 1.3 collective-permute-done.17.refs_12_
  69.1 1.8 collective-permute-start.39
  70.9 1.2 collective-permute-done.37.refs_10_
  72.1 1.2 collective-permute-start.41
  73.8 4.3 %collective-permute-done.33.refs_6_ = bf16[64,2176]{1,0:T(8,128)(2,1)S(1)} collective-permute-done((bf16[64,2176]{1,0:T(8,128)(2,1)S(1)}, bf16[64,2176]{1,0:T(8,128)(2,1)S(1)}, u32[]{:S(2)}, u32[]{:S(2)}) %collective-permute-start.33) | collective-permute-done | bytes 278560 | tf_op jit(solution)/shard_map/ppermute | solution.py:367
  78.1 0.5 collective-permute-start.38
  78.7 5.4 %collective-permute-done.41.refs_14_ = bf16[64,2176]{1,0:T(8,128)(2,1)S(1)} collective-permute-done((bf16[64,2176]{1,0:T(8,128)(2,1)S(1)}, bf16[64,2176]{1,0:T(8,128)(2,1)S(1)}, u32[]{:S(2)}, u32[]{:S(2)}) %collective-permute-start.41) | collective-permute-done | bytes 278560 | tf_op jit(solution)/shard_map/ppermute | solution.py:367
  84.2 0.6 collective-permute-start.14
  84.9 0.5 collective-permute-start.12
  86.1 0.7 copy-done.34
  87.0 12.2 %up_kernel.3 = (bf16[8,128,256]{2,1,0:T(8,128)(2,1)}, bf16[4,256,256]{2,1,0:T(8,128)(2,1)S(1)}) custom-call(s32[2]{0:T(128)S(1)} %pad_add_fusion.where_ref, bf16[64,2176]{1,0:T(8,128)(2,1)} %copy-done.18, bf16[64,2176]{1,0:T(8,128)(2,1)} %collective-permute-done.28.refs_1_, bf16[64,2176]{1,0:T(8,128)(2,1)} %copy-done.21, bf16[64,2176]{1,0:T(8,128)(2,1)} %copy-done.24, ...), custom_call_target="tpu_custom_call" | custom-call | tf_op jit(solution)/shard_map/up_kernel/pallas_call | solution.py:466
  99.2 1.6 collective-permute-start.44
  100.8 14.1 %up_kernel.2 = (bf16[10,128,256]{2,1,0:T(8,128)(2,1)S(1)}, bf16[4,256,256]{2,1,0:T(8,128)(2,1)S(1)}) custom-call(s32[2]{0:T(128)S(1)} %pad_add_fusion.where_ref, bf16[64,2176]{1,0:T(8,128)(2,1)} %copy-done.13, bf16[64,2176]{1,0:T(8,128)(2,1)} %copy-done.14, bf16[64,2176]{1,0:T(8,128)(2,1)} %copy-done.15, bf16[64,2176]{1,0:T(8,128)(2,1)} %copy-done.19, ...), custom_call_target="tpu_custom_call" | custom-call | tf_op jit(solution)/shard_map/up_kernel/pallas_call | solution.py:466
  115.0 0.6 collective-permute-start.22
  115.6 0.5 collective-permute-start.45
  116.1 15.8 %collective-permute-done.22.refs_2_ = bf16[10,128,256]{2,1,0:T(8,128)(2,1)S(1)} collective-permute-done((bf16[10,128,256]{2,1,0:T(8,128)(2,1)S(1)}, bf16[10,128,256]{2,1,0:T(8,128)(2,1)S(1)}, u32[]{:S(2)}, u32[]{:S(2)}) %collective-permute-start.22) | collective-permute-done | bytes 655392 | tf_op jit(solution)/shard_map/ppermute | solution.py:367
  131.9 1.7 constant_dynamic-slice_fusion.2
  133.6 0.5 collective-permute-start.4
  134.1 1.0 copy-done.2
  135.2 6.7 %down_kernel.3 = (bf16[256,512]{1,0:T(8,128)(2,1)S(1)}, bf16[256,512]{1,0:T(8,128)(2,1)S(1)}, bf16[256,512]{1,0:T(8,128)(2,1)S(1)}, bf16[256,512]{1,0:T(8,128)(2,1)}) custom-call(s32[2]{0:T(128)S(1)} %pad_add_fusion.where_ref, bf16[8,128,256]{2,1,0:T(8,128)(2,1)} %get-tuple-element.25.refs_0_, bf16[8,128,256]{2,1,0:T(8,128)(2,1)} %collective-permute-done.43.refs_1_, ...), custom_call_target="tpu_custom_call" | custom-call | tf_op jit(solution)/shard_map/down_kernel/pallas_call | solution.py:502
  141.8 0.7 copy-done.5
  142.5 0.7 copy-done.7
  143.2 0.7 copy-done.9
  143.9 1.7 collective-permute-start.47
  145.7 0.6 broadcast_in_dim.56
  146.3 0.7 broadcast_in_dim.57
  147.0 1.0 fusion.17
  148.1 7.5 %down_kernel.2 = (f32[256,512]{1,0:T(8,128)S(1)}, bf16[256,512]{1,0:T(8,128)(2,1)S(1)}, bf16[256,512]{1,0:T(8,128)(2,1)}, bf16[256,512]{1,0:T(8,128)(2,1)S(1)}, bf16[256,512]{1,0:T(8,128)(2,1)S(1)}) custom-call(s32[2]{0:T(128)S(1)} %pad_add_fusion.where_ref, bf16[10,128,256]{2,1,0:T(8,128)(2,1)S(1)} %get-tuple-element.18.refs_0_, ...), custom_call_target="tpu_custom_call" | custom-call | tf_op jit(solution)/shard_map/down_kernel/pallas_call | solution.py:502
  156.0 1.7 collective-permute-start.46
  157.7 1.0 add_convert_fusion.2
  159.2 5.7 %collective-permute-done.25 = bf16[256,512]{1,0:T(8,128)(2,1)S(1)} collective-permute-done((bf16[256,512]{1,0:T(8,128)(2,1)S(1)}, bf16[256,512]{1,0:T(8,128)(2,1)S(1)}, u32[]{:S(2)}, u32[]{:S(2)}) %collective-permute-start.25) | collective-permute-done | bytes 262176 | tf_op jit(solution)/shard_map/ppermute | solution.py:367
  165.0 5.5 %collective-permute-done.46 = bf16[256,512]{1,0:T(8,128)(2,1)S(1)} collective-permute-done((bf16[256,512]{1,0:T(8,128)(2,1)S(1)}, bf16[256,512]{1,0:T(8,128)(2,1)S(1)}, u32[]{:S(2)}, u32[]{:S(2)}) %collective-permute-start.46) | collective-permute-done | bytes 262176 | tf_op jit(solution)/shard_map/ppermute | solution.py:367
  170.8 0.6 gather_fusion
  171.3 4.3 %collective-permute-done.24 = bf16[256,512]{1,0:T(8,128)(2,1)S(1)} collective-permute-done((bf16[256,512]{1,0:T(8,128)(2,1)}, bf16[256,512]{1,0:T(8,128)(2,1)S(1)}, u32[]{:S(2)}, u32[]{:S(2)}) %collective-permute-start.24) | collective-permute-done | bytes 262176 | tf_op jit(solution)/shard_map/ppermute | solution.py:367
  175.6 7.8 %collective-permute-done.49 = bf16[256,512]{1,0:T(8,128)(2,1)S(1)} collective-permute-done((bf16[256,512]{1,0:T(8,128)(2,1)S(1)}, bf16[256,512]{1,0:T(8,128)(2,1)S(1)}, u32[]{:S(2)}, u32[]{:S(2)}) %collective-permute-start.49) | collective-permute-done | bytes 262176 | tf_op jit(solution)/shard_map/ppermute | solution.py:367
  183.4 2.0 %add_convert_fusion = bf16[256,512]{1,0:T(8,128)(2,1)} fusion(bf16[256,512]{1,0:T(8,128)(2,1)S(1)} %collective-permute-done.49, bf16[256,512]{1,0:T(8,128)(2,1)S(1)} %collective-permute-done.26, bf16[256,512]{1,0:T(8,128)(2,1)S(1)} %collective-permute-done.24, bf16[256,512]{1,0:T(8,128)(2,1)} %copy-done.4, f32[256,512]{1,0:T(8,128)} %copy-done.3, ...), kind=kLoop, calls=%fused_computation.22 | loop fusion | flops 1572864 | bytes 2097408 | tf_op jit(solution)/shard_map/convert_element_type | solution.py:534
  (170 shorter events, 7.0 us)
Async XLA Ops:
  1.2 8.0 %collective-permute-start = (bf16[128,128]{1,0:T(8,128)(2,1)S(1)}, bf16[128,128]{1,0:T(8,128)(2,1)S(1)}, u32[]{:S(2)}, u32[]{:S(2)}) collective-permute-start(bf16[128,128]{1,0:T(8,128)(2,1)S(1)} %get-tuple-element.44), channel_id=1, source_target_pairs={{0,4},{4,8},{8,12},{12,16},{16,20},{20,24},{24,28},{1,5},{5,9},{9,... | collective-permute-start | bytes 98312 | tf_op jit(solution)/shard_map/ppermute | solution.py:35
  6.1 5.8 %collective-permute-start.1 = (bf16[128,128]{1,0:T(8,128)(2,1)S(1)}, bf16[128,128]{1,0:T(8,128)(2,1)S(1)}, u32[]{:S(2)}, u32[]{:S(2)}) collective-permute-start(bf16[128,128]{1,0:T(8,128)(2,1)S(1)} %get-tuple-element.45), channel_id=1, source_target_pairs={{4,0},{8,4},{12,8},{16,12},{20,16},{24,20},{28,24},{5,1},{9,5},{13... | collective-permute-start | bytes 98312 | tf_op jit(solution)/shard_map/ppermute | solution.py:36
  15.2 2.3 %collective-permute-start.2 = (bf16[2,64,2048]{2,1,0:T(8,128)(2,1)}, bf16[2,64,2048]{2,1,0:T(8,128)(2,1)}, u32[]{:S(2)}, u32[]{:S(2)}) collective-permute-start(bf16[2,64,2048]{2,1,0:T(8,128)(2,1)} %fusion.8), channel_id=1, source_target_pairs={{0,1},{1,0},{2,3},{3,2},{4,5},{5,4},{6,7},{7,6},{8,9},{9,8},{10,11... | collective-permute-start | bytes 1572872 | tf_op jit(solution)/shard_map/ppermute | solution.py:367
  19.6 8.4 %collective-permute-start.3 = (bf16[64,2048]{1,0:T(8,128)(2,1)S(1)}, bf16[64,2048]{1,0:T(8,128)(2,1)S(1)}, u32[]{:S(2)}, u32[]{:S(2)}) collective-permute-start(bf16[64,2048]{1,0:T(8,128)(2,1)S(1)} %fusion.13), channel_id=1, source_target_pairs={{0,2},{1,3},{2,0},{3,1},{4,6},{5,7},{6,4},{7,5},{8,10},{9,11},{10,... | collective-permute-start | bytes 786440 | tf_op jit(solution)/shard_map/ppermute | solution.py:367
  30.2 68.9 %copy-start.13 = (bf16[64,2176]{1,0:T(8,128)(2,1)}, bf16[64,2176]{1,0:T(8,128)(2,1)S(1)}, u32[]{:S(2)}) copy-start(bf16[64,2176]{1,0:T(8,128)(2,1)S(1)} %concatenate.27.refs_0_) | copy-start | bytes 835588
  30.2 14.9 %collective-permute-start.27 = (bf16[64,2176]{1,0:T(8,128)(2,1)S(1)}, bf16[64,2176]{1,0:T(8,128)(2,1)S(1)}, u32[]{:S(2)}, u32[]{:S(2)}) collective-permute-start(bf16[64,2176]{1,0:T(8,128)(2,1)S(1)} %concatenate.27.refs_0_), channel_id=1, source_target_pairs={{0,16},{4,20},{8,24},{12,28},{16,0},{20,4},{24,8},{28,12},{1,17},{... | collective-permute-start | bytes 835592 | tf_op jit(solution)/shard_map/ppermute | solution.py:367
  32.9 12.2 %collective-permute-start.6 = (bf16[64,2176]{1,0:T(8,128)(2,1)S(1)}, bf16[64,2176]{1,0:T(8,128)(2,1)S(1)}, u32[]{:S(2)}, u32[]{:S(2)}) collective-permute-start(bf16[64,2176]{1,0:T(8,128)(2,1)S(1)} %concatenate.27.refs_0_), channel_id=1, source_target_pairs={{0,1},{1,0},{2,3},{3,2},{4,5},{5,4},{6,7},{7,6},{8,9},{9,8},{10,11... | collective-permute-start | bytes 835592 | tf_op jit(solution)/shard_map/ppermute | solution.py:367
  32.9 13.8 %collective-permute-start.7 = (bf16[64,2176]{1,0:T(8,128)(2,1)S(1)}, bf16[64,2176]{1,0:T(8,128)(2,1)S(1)}, u32[]{:S(2)}, u32[]{:S(2)}) collective-permute-start(bf16[64,2176]{1,0:T(8,128)(2,1)S(1)} %concatenate.27.refs_0_), channel_id=1, source_target_pairs={{0,2},{1,3},{2,0},{3,1},{4,6},{5,7},{6,4},{7,5},{8,10},{9,11},{10,... | collective-permute-start | bytes 835592 | tf_op jit(solution)/shard_map/ppermute | solution.py:367
  34.4 14.8 %collective-permute-start.9 = (bf16[64,2176]{1,0:T(8,128)(2,1)S(1)}, bf16[64,2176]{1,0:T(8,128)(2,1)S(1)}, u32[]{:S(2)}, u32[]{:S(2)}) collective-permute-start(bf16[64,2176]{1,0:T(8,128)(2,1)S(1)} %concatenate.27.refs_0_), channel_id=1, source_target_pairs={{0,4},{4,0},{8,12},{12,8},{16,20},{20,16},{24,28},{28,24},{1,5},{5... | collective-permute-start | bytes 835592 | tf_op jit(solution)/shard_map/ppermute | solution.py:367
  36.8 13.3 %collective-permute-start.13 = (bf16[64,2176]{1,0:T(8,128)(2,1)S(1)}, bf16[64,2176]{1,0:T(8,128)(2,1)S(1)}, u32[]{:S(2)}, u32[]{:S(2)}) collective-permute-start(bf16[64,2176]{1,0:T(8,128)(2,1)S(1)} %concatenate.27.refs_0_), channel_id=1, source_target_pairs={{0,8},{4,12},{8,0},{12,4},{16,24},{20,28},{24,16},{28,20},{1,9},{5... | collective-permute-start | bytes 835592 | tf_op jit(solution)/shard_map/ppermute | solution.py:367
  45.1 41.9 %copy-start.18 = (bf16[64,2176]{1,0:T(8,128)(2,1)}, bf16[64,2176]{1,0:T(8,128)(2,1)S(1)}, u32[]{:S(2)}) copy-start(bf16[64,2176]{1,0:T(8,128)(2,1)S(1)} %collective-permute-done.27.refs_0_) | copy-start | bytes 835588
  45.1 5.1 %collective-permute-start.28 = (bf16[64,2176]{1,0:T(8,128)(2,1)S(1)}, bf16[64,2176]{1,0:T(8,128)(2,1)}, u32[]{:S(2)}, u32[]{:S(2)}) collective-permute-start(bf16[64,2176]{1,0:T(8,128)(2,1)S(1)} %collective-permute-done.27.refs_0_), channel_id=1, source_target_pairs={{0,1},{1,0},{2,3},{3,2},{4,5},{5,4},{6,7},{7,6},{8,9},{9,8},{10,11... | collective-permute-start | bytes 835592 | tf_op jit(solution)/shard_map/ppermute | solution.py:367
  45.1 54.0 %copy-start.14 = (bf16[64,2176]{1,0:T(8,128)(2,1)}, bf16[64,2176]{1,0:T(8,128)(2,1)S(1)}, u32[]{:S(2)}) copy-start(bf16[64,2176]{1,0:T(8,128)(2,1)S(1)} %collective-permute-done.6.refs_1_) | copy-start | bytes 835588
  45.1 9.1 %collective-permute-start.29 = (bf16[64,2176]{1,0:T(8,128)(2,1)S(1)}, bf16[64,2176]{1,0:T(8,128)(2,1)S(1)}, u32[]{:S(2)}, u32[]{:S(2)}) collective-permute-start(bf16[64,2176]{1,0:T(8,128)(2,1)S(1)} %collective-permute-done.27.refs_0_), channel_id=1, source_target_pairs={{0,2},{1,3},{2,0},{3,1},{4,6},{5,7},{6,4},{7,5},{8,10},{9,11},{10,... | collective-permute-start | bytes 835592 | tf_op jit(solution)/shard_map/ppermute | solution.py:367
  46.7 52.5 %copy-start.15 = (bf16[64,2176]{1,0:T(8,128)(2,1)}, bf16[64,2176]{1,0:T(8,128)(2,1)S(1)}, u32[]{:S(2)}) copy-start(bf16[64,2176]{1,0:T(8,128)(2,1)S(1)} %collective-permute-done.7.refs_2_) | copy-start | bytes 835588
  46.7 9.9 %collective-permute-start.31 = (bf16[64,2176]{1,0:T(8,128)(2,1)S(1)}, bf16[64,2176]{1,0:T(8,128)(2,1)S(1)}, u32[]{:S(2)}, u32[]{:S(2)}) collective-permute-start(bf16[64,2176]{1,0:T(8,128)(2,1)S(1)} %collective-permute-done.27.refs_0_), channel_id=1, source_target_pairs={{0,4},{4,0},{8,12},{12,8},{16,20},{20,16},{24,28},{28,24},{1,5},{5... | collective-permute-start | bytes 835592 | tf_op jit(solution)/shard_map/ppermute | solution.py:367
  49.2 50.0 %copy-start.16 = (bf16[64,2176]{1,0:T(8,128)(2,1)}, bf16[64,2176]{1,0:T(8,128)(2,1)S(1)}, u32[]{:S(2)}) copy-start(bf16[64,2176]{1,0:T(8,128)(2,1)S(1)} %collective-permute-done.9.refs_4_) | copy-start | bytes 835588
  49.2 9.0 %collective-permute-start.35 = (bf16[64,2176]{1,0:T(8,128)(2,1)S(1)}, bf16[64,2176]{1,0:T(8,128)(2,1)S(1)}, u32[]{:S(2)}, u32[]{:S(2)}) collective-permute-start(bf16[64,2176]{1,0:T(8,128)(2,1)S(1)} %collective-permute-done.27.refs_0_), channel_id=1, source_target_pairs={{0,8},{4,12},{8,0},{12,4},{16,24},{20,28},{24,16},{28,20},{1,9},{5... | collective-permute-start | bytes 835592 | tf_op jit(solution)/shard_map/ppermute | solution.py:367
  50.1 49.0 %copy-start.17 = (bf16[64,2176]{1,0:T(8,128)(2,1)}, bf16[64,2176]{1,0:T(8,128)(2,1)S(1)}, u32[]{:S(2)}) copy-start(bf16[64,2176]{1,0:T(8,128)(2,1)S(1)} %collective-permute-done.13.refs_8_) | copy-start | bytes 835588
  50.2 8.2 %collective-permute-start.8 = (bf16[64,2176]{1,0:T(8,128)(2,1)S(1)}, bf16[64,2176]{1,0:T(8,128)(2,1)S(1)}, u32[]{:S(2)}, u32[]{:S(2)}) collective-permute-start(bf16[64,2176]{1,0:T(8,128)(2,1)S(1)} %collective-permute-done.7.refs_2_), channel_id=1, source_target_pairs={{0,1},{1,0},{2,3},{3,2},{4,5},{5,4},{6,7},{7,6},{8,9},{9,8},{10,11... | collective-permute-start | bytes 835592 | tf_op jit(solution)/shard_map/ppermute | solution.py:367
  50.2 8.2 %collective-permute-start.10 = (bf16[64,2176]{1,0:T(8,128)(2,1)S(1)}, bf16[64,2176]{1,0:T(8,128)(2,1)S(1)}, u32[]{:S(2)}, u32[]{:S(2)}) collective-permute-start(bf16[64,2176]{1,0:T(8,128)(2,1)S(1)} %collective-permute-done.9.refs_4_), channel_id=1, source_target_pairs={{0,1},{1,0},{2,3},{3,2},{4,5},{5,4},{6,7},{7,6},{8,9},{9,8},{10,11... | collective-permute-start | bytes 835592 | tf_op jit(solution)/shard_map/ppermute | solution.py:367
  54.2 30.0 %copy-start.21 = (bf16[64,2176]{1,0:T(8,128)(2,1)}, bf16[64,2176]{1,0:T(8,128)(2,1)S(1)}, u32[]{:S(2)}) copy-start(bf16[64,2176]{1,0:T(8,128)(2,1)S(1)} %collective-permute-done.29.refs_2_) | copy-start | bytes 835588
  54.2 10.0 %collective-permute-start.11 = (bf16[64,2176]{1,0:T(8,128)(2,1)S(1)}, bf16[64,2176]{1,0:T(8,128)(2,1)}, u32[]{:S(2)}, u32[]{:S(2)}) collective-permute-start(bf16[64,2176]{1,0:T(8,128)(2,1)S(1)} %collective-permute-done.7.refs_2_), channel_id=1, source_target_pairs={{0,4},{4,0},{8,12},{12,8},{16,20},{20,16},{24,28},{28,24},{1,5},{5... | collective-permute-start | bytes 835592 | tf_op jit(solution)/shard_map/ppermute | solution.py:367
  56.6 27.5 %copy-start.22 = (bf16[64,2176]{1,0:T(8,128)(2,1)}, bf16[64,2176]{1,0:T(8,128)(2,1)S(1)}, u32[]{:S(2)}) copy-start(bf16[64,2176]{1,0:T(8,128)(2,1)S(1)} %collective-permute-done.31.refs_4_) | copy-start | bytes 835588
  56.6 9.6 %collective-permute-start.15 = (bf16[64,2176]{1,0:T(8,128)(2,1)S(1)}, bf16[64,2176]{1,0:T(8,128)(2,1)}, u32[]{:S(2)}, u32[]{:S(2)}) collective-permute-start(bf16[64,2176]{1,0:T(8,128)(2,1)S(1)} %collective-permute-done.13.refs_8_), channel_id=1, source_target_pairs={{0,2},{1,3},{2,0},{3,1},{4,6},{5,7},{6,4},{7,5},{8,10},{9,11},{10,... | collective-permute-start | bytes 835592 | tf_op jit(solution)/shard_map/ppermute | solution.py:367
  58.2 26.6 %copy-start.23 = (bf16[64,2176]{1,0:T(8,128)(2,1)}, bf16[64,2176]{1,0:T(8,128)(2,1)S(1)}, u32[]{:S(2)}) copy-start(bf16[64,2176]{1,0:T(8,128)(2,1)S(1)} %collective-permute-done.35.refs_8_) | copy-start | bytes 835588
  58.2 10.9 %collective-permute-start.17 = (bf16[64,2176]{1,0:T(8,128)(2,1)S(1)}, bf16[64,2176]{1,0:T(8,128)(2,1)}, u32[]{:S(2)}, u32[]{:S(2)}) collective-permute-start(bf16[64,2176]{1,0:T(8,128)(2,1)S(1)} %collective-permute-done.13.refs_8_), channel_id=1, source_target_pairs={{0,4},{4,0},{8,12},{12,8},{16,20},{20,16},{24,28},{28,24},{1,5},{5... | collective-permute-start | bytes 835592 | tf_op jit(solution)/shard_map/ppermute | solution.py:367
  58.4 40.8 %copy-start.19 = (bf16[64,2176]{1,0:T(8,128)(2,1)}, bf16[64,2176]{1,0:T(8,128)(2,1)S(1)}, u32[]{:S(2)}) copy-start(bf16[64,2176]{1,0:T(8,128)(2,1)S(1)} %collective-permute-done.8.refs_3_) | copy-start | bytes 835588
  58.4 10.7 %collective-permute-start.30 = (bf16[64,2176]{1,0:T(8,128)(2,1)S(1)}, bf16[64,2176]{1,0:T(8,128)(2,1)S(1)}, u32[]{:S(2)}, u32[]{:S(2)}) collective-permute-start(bf16[64,2176]{1,0:T(8,128)(2,1)S(1)} %collective-permute-done.29.refs_2_), channel_id=1, source_target_pairs={{0,1},{1,0},{2,3},{3,2},{4,5},{5,4},{6,7},{7,6},{8,9},{9,8},{10,11... | collective-permute-start | bytes 835592 | tf_op jit(solution)/shard_map/ppermute | solution.py:367
  58.4 40.8 %copy-start.20 = (bf16[64,2176]{1,0:T(8,128)(2,1)}, bf16[64,2176]{1,0:T(8,128)(2,1)S(1)}, u32[]{:S(2)}) copy-start(bf16[64,2176]{1,0:T(8,128)(2,1)S(1)} %collective-permute-done.10.refs_5_) | copy-start | bytes 835588
  58.4 13.7 %collective-permute-start.37 = (bf16[64,2176]{1,0:T(8,128)(2,1)S(1)}, bf16[64,2176]{1,0:T(8,128)(2,1)S(1)}, u32[]{:S(2)}, u32[]{:S(2)}) collective-permute-start(bf16[64,2176]{1,0:T(8,128)(2,1)S(1)} %collective-permute-done.35.refs_8_), channel_id=1, source_target_pairs={{0,2},{1,3},{2,0},{3,1},{4,6},{5,7},{6,4},{7,5},{8,10},{9,11},{10,... | collective-permute-start | bytes 835592 | tf_op jit(solution)/shard_map/ppermute | solution.py:367
  64.2 9.1 %collective-permute-start.32 = (bf16[64,2176]{1,0:T(8,128)(2,1)S(1)}, bf16[64,2176]{1,0:T(8,128)(2,1)S(1)}, u32[]{:S(2)}, u32[]{:S(2)}) collective-permute-start(bf16[64,2176]{1,0:T(8,128)(2,1)S(1)} %collective-permute-done.31.refs_4_), channel_id=1, source_target_pairs={{0,1},{1,0},{2,3},{3,2},{4,5},{5,4},{6,7},{7,6},{8,9},{9,8},{10,11... | collective-permute-start | bytes 835592 | tf_op jit(solution)/shard_map/ppermute | solution.py:367
  66.3 11.8 %collective-permute-start.33 = (bf16[64,2176]{1,0:T(8,128)(2,1)S(1)}, bf16[64,2176]{1,0:T(8,128)(2,1)S(1)}, u32[]{:S(2)}, u32[]{:S(2)}) collective-permute-start(bf16[64,2176]{1,0:T(8,128)(2,1)S(1)} %collective-permute-done.31.refs_4_), channel_id=1, source_target_pairs={{0,2},{1,3},{2,0},{3,1},{4,6},{5,7},{6,4},{7,5},{8,10},{9,11},{10,... | collective-permute-start | bytes 835592 | tf_op jit(solution)/shard_map/ppermute | solution.py:367
  69.1 9.0 %collective-permute-start.36 = (bf16[64,2176]{1,0:T(8,128)(2,1)S(1)}, bf16[64,2176]{1,0:T(8,128)(2,1)S(1)}, u32[]{:S(2)}, u32[]{:S(2)}) collective-permute-start(bf16[64,2176]{1,0:T(8,128)(2,1)S(1)} %collective-permute-done.35.refs_8_), channel_id=1, source_target_pairs={{0,1},{1,0},{2,3},{3,2},{4,5},{5,4},{6,7},{7,6},{8,9},{9,8},{10,11... | collective-permute-start | bytes 835592 | tf_op jit(solution)/shard_map/ppermute | solution.py:367
  69.1 15.6 %copy-start.24 = (bf16[64,2176]{1,0:T(8,128)(2,1)}, bf16[64,2176]{1,0:T(8,128)(2,1)S(1)}, u32[]{:S(2)}) copy-start(bf16[64,2176]{1,0:T(8,128)(2,1)S(1)} %collective-permute-done.30.refs_3_) | copy-start | bytes 835588
  69.1 9.6 %collective-permute-start.39 = (bf16[64,2176]{1,0:T(8,128)(2,1)S(1)}, bf16[64,2176]{1,0:T(8,128)(2,1)S(1)}, u32[]{:S(2)}, u32[]{:S(2)}) collective-permute-start(bf16[64,2176]{1,0:T(8,128)(2,1)S(1)} %collective-permute-done.35.refs_8_), channel_id=1, source_target_pairs={{0,4},{4,0},{8,12},{12,8},{16,20},{20,16},{24,28},{28,24},{1,5},{5... | collective-permute-start | bytes 835592 | tf_op jit(solution)/shard_map/ppermute | solution.py:367
  72.1 12.0 %collective-permute-start.41 = (bf16[64,2176]{1,0:T(8,128)(2,1)S(1)}, bf16[64,2176]{1,0:T(8,128)(2,1)S(1)}, u32[]{:S(2)}, u32[]{:S(2)}) collective-permute-start(bf16[64,2176]{1,0:T(8,128)(2,1)S(1)} %collective-permute-done.37.refs_10_), channel_id=1, source_target_pairs={{0,4},{4,0},{8,12},{12,8},{16,20},{20,16},{24,28},{28,24},{1,5},{5... | collective-permute-start | bytes 835592 | tf_op jit(solution)/shard_map/ppermute | solution.py:367
  73.4 10.8 %collective-permute-start.19 = (bf16[64,2176]{1,0:T(8,128)(2,1)}, bf16[64,2176]{1,0:T(8,128)(2,1)}, u32[]{:S(2)}, u32[]{:S(2)}) collective-permute-start(bf16[64,2176]{1,0:T(8,128)(2,1)} %collective-permute-done.17.refs_12_), channel_id=1, source_target_pairs={{0,2},{1,3},{2,0},{3,1},{4,6},{5,7},{6,4},{7,5},{8,10},{9,11},{10,... | collective-permute-start | bytes 835592 | tf_op jit(solution)/shard_map/ppermute | solution.py:367
  78.1 6.6 %collective-permute-start.34 = (bf16[64,2176]{1,0:T(8,128)(2,1)S(1)}, bf16[64,2176]{1,0:T(8,128)(2,1)S(1)}, u32[]{:S(2)}, u32[]{:S(2)}) collective-permute-start(bf16[64,2176]{1,0:T(8,128)(2,1)S(1)} %collective-permute-done.33.refs_6_), channel_id=1, source_target_pairs={{0,1},{1,0},{2,3},{3,2},{4,5},{5,4},{6,7},{7,6},{8,9},{9,8},{10,11... | collective-permute-start | bytes 835592 | tf_op jit(solution)/shard_map/ppermute | solution.py:367
  78.1 6.7 %collective-permute-start.38 = (bf16[64,2176]{1,0:T(8,128)(2,1)S(1)}, bf16[64,2176]{1,0:T(8,128)(2,1)S(1)}, u32[]{:S(2)}, u32[]{:S(2)}) collective-permute-start(bf16[64,2176]{1,0:T(8,128)(2,1)S(1)} %collective-permute-done.37.refs_10_), channel_id=1, source_target_pairs={{0,1},{1,0},{2,3},{3,2},{4,5},{5,4},{6,7},{7,6},{8,9},{9,8},{10,11... | collective-permute-start | bytes 835592 | tf_op jit(solution)/shard_map/ppermute | solution.py:367
  78.7 6.7 %collective-permute-start.40 = (bf16[64,2176]{1,0:T(8,128)(2,1)S(1)}, bf16[64,2176]{1,0:T(8,128)(2,1)S(1)}, u32[]{:S(2)}, u32[]{:S(2)}) collective-permute-start(bf16[64,2176]{1,0:T(8,128)(2,1)S(1)} %collective-permute-done.39.refs_12_), channel_id=1, source_target_pairs={{0,1},{1,0},{2,3},{3,2},{4,5},{5,4},{6,7},{7,6},{8,9},{9,8},{10,11... | collective-permute-start | bytes 835592 | tf_op jit(solution)/shard_map/ppermute | solution.py:367
  84.1 1.6 collective-permute-start.42
  84.2 15.1 %collective-permute-start.14 = (bf16[64,2176]{1,0:T(8,128)(2,1)S(1)}, bf16[64,2176]{1,0:T(8,128)(2,1)}, u32[]{:S(2)}, u32[]{:S(2)}) collective-permute-start(bf16[64,2176]{1,0:T(8,128)(2,1)S(1)} %collective-permute-done.13.refs_8_), channel_id=1, source_target_pairs={{0,1},{1,0},{2,3},{3,2},{4,5},{5,4},{6,7},{7,6},{8,9},{9,8},{10,11... | collective-permute-start | bytes 835592 | tf_op jit(solution)/shard_map/ppermute | solution.py:367
  84.7 16.1 %collective-permute-start.18 = (bf16[64,2176]{1,0:T(8,128)(2,1)}, bf16[64,2176]{1,0:T(8,128)(2,1)}, u32[]{:S(2)}, u32[]{:S(2)}) collective-permute-start(bf16[64,2176]{1,0:T(8,128)(2,1)} %collective-permute-done.17.refs_12_), channel_id=1, source_target_pairs={{0,1},{1,0},{2,3},{3,2},{4,5},{5,4},{6,7},{7,6},{8,9},{9,8},{10,11... | collective-permute-start | bytes 835592 | tf_op jit(solution)/shard_map/ppermute | solution.py:367
  84.9 16.0 %collective-permute-start.12 = (bf16[64,2176]{1,0:T(8,128)(2,1)}, bf16[64,2176]{1,0:T(8,128)(2,1)}, u32[]{:S(2)}, u32[]{:S(2)}) collective-permute-start(bf16[64,2176]{1,0:T(8,128)(2,1)} %collective-permute-done.11.refs_6_), channel_id=1, source_target_pairs={{0,1},{1,0},{2,3},{3,2},{4,5},{5,4},{6,7},{7,6},{8,9},{9,8},{10,11... | collective-permute-start | bytes 835592 | tf_op jit(solution)/shard_map/ppermute | solution.py:367
  85.4 15.4 %collective-permute-start.16 = (bf16[64,2176]{1,0:T(8,128)(2,1)}, bf16[64,2176]{1,0:T(8,128)(2,1)}, u32[]{:S(2)}, u32[]{:S(2)}) collective-permute-start(bf16[64,2176]{1,0:T(8,128)(2,1)} %collective-permute-done.15.refs_10_), channel_id=1, source_target_pairs={{0,1},{1,0},{2,3},{3,2},{4,5},{5,4},{6,7},{7,6},{8,9},{9,8},{10,11... | collective-permute-start | bytes 835592 | tf_op jit(solution)/shard_map/ppermute | solution.py:367
  86.8 14.0 %collective-permute-start.20 = (bf16[64,2176]{1,0:T(8,128)(2,1)}, bf16[64,2176]{1,0:T(8,128)(2,1)}, u32[]{:S(2)}, u32[]{:S(2)}) collective-permute-start(bf16[64,2176]{1,0:T(8,128)(2,1)} %collective-permute-done.19.refs_14_), channel_id=1, source_target_pairs={{0,1},{1,0},{2,3},{3,2},{4,5},{5,4},{6,7},{7,6},{8,9},{9,8},{10,11... | collective-permute-start | bytes 835592 | tf_op jit(solution)/shard_map/ppermute | solution.py:367
  99.2 15.8 %copy-start.1 = (bf16[4,256,256]{2,1,0:T(8,128)(2,1)}, bf16[4,256,256]{2,1,0:T(8,128)(2,1)S(1)}, u32[]{:S(2)}) copy-start(bf16[4,256,256]{2,1,0:T(8,128)(2,1)S(1)} %get-tuple-element.26.refs_4_) | copy-start | bytes 1572868
  99.2 16.3 %collective-permute-start.44 = (bf16[8,128,256]{2,1,0:T(8,128)(2,1)}, bf16[8,128,256]{2,1,0:T(8,128)(2,1)}, u32[]{:S(2)}, u32[]{:S(2)}) collective-permute-start(bf16[8,128,256]{2,1,0:T(8,128)(2,1)} %get-tuple-element.25.refs_0_), channel_id=1, source_target_pairs={{0,2},{1,3},{2,0},{3,1},{4,6},{5,7},{6,4},{7,5},{8,10},{9,11},{10,... | collective-permute-start | bytes 1572872 | tf_op jit(solution)/shard_map/ppermute | solution.py:367
  115.0 16.9 %collective-permute-start.22 = (bf16[10,128,256]{2,1,0:T(8,128)(2,1)S(1)}, bf16[10,128,256]{2,1,0:T(8,128)(2,1)S(1)}, u32[]{:S(2)}, u32[]{:S(2)}) collective-permute-start(bf16[10,128,256]{2,1,0:T(8,128)(2,1)S(1)} %get-tuple-element.18.refs_0_), channel_id=1, source_target_pairs={{0,2},{1,3},{2,0},{3,1},{4,6},{5,7},{6,4},{7,5},{8,10},{9,11},{10,... | collective-permute-start | bytes 1966088 | tf_op jit(solution)/shard_map/ppermute | solution.py:367
  115.6 18.6 %collective-permute-start.43 = (bf16[8,128,256]{2,1,0:T(8,128)(2,1)}, bf16[8,128,256]{2,1,0:T(8,128)(2,1)}, u32[]{:S(2)}, u32[]{:S(2)}) collective-permute-start(bf16[8,128,256]{2,1,0:T(8,128)(2,1)} %get-tuple-element.25.refs_0_), channel_id=1, source_target_pairs={{0,1},{1,0},{2,3},{3,2},{4,5},{5,4},{6,7},{7,6},{8,9},{9,8},{10,11... | collective-permute-start | bytes 1572872 | tf_op jit(solution)/shard_map/ppermute | solution.py:367
  115.6 18.5 %collective-permute-start.45 = (bf16[8,128,256]{2,1,0:T(8,128)(2,1)}, bf16[8,128,256]{2,1,0:T(8,128)(2,1)}, u32[]{:S(2)}, u32[]{:S(2)}) collective-permute-start(bf16[8,128,256]{2,1,0:T(8,128)(2,1)} %collective-permute-done.44.refs_2_), channel_id=1, source_target_pairs={{0,1},{1,0},{2,3},{3,2},{4,5},{5,4},{6,7},{7,6},{8,9},{9,8},{10,11... | collective-permute-start | bytes 1572872 | tf_op jit(solution)/shard_map/ppermute | solution.py:367
  116.1 32.0 %collective-permute-start.21 = (bf16[10,128,256]{2,1,0:T(8,128)(2,1)S(1)}, bf16[10,128,256]{2,1,0:T(8,128)(2,1)S(1)}, u32[]{:S(2)}, u32[]{:S(2)}) collective-permute-start(bf16[10,128,256]{2,1,0:T(8,128)(2,1)S(1)} %get-tuple-element.18.refs_0_), channel_id=1, source_target_pairs={{0,1},{1,0},{2,3},{3,2},{4,5},{5,4},{6,7},{7,6},{8,9},{9,8},{10,11... | collective-permute-start | bytes 1966088 | tf_op jit(solution)/shard_map/ppermute | solution.py:367
  131.9 16.2 %collective-permute-start.23 = (bf16[10,128,256]{2,1,0:T(8,128)(2,1)S(1)}, bf16[10,128,256]{2,1,0:T(8,128)(2,1)}, u32[]{:S(2)}, u32[]{:S(2)}) collective-permute-start(bf16[10,128,256]{2,1,0:T(8,128)(2,1)S(1)} %collective-permute-done.22.refs_2_), channel_id=1, source_target_pairs={{0,1},{1,0},{2,3},{3,2},{4,5},{5,4},{6,7},{7,6},{8,9},{9,8},{10,11... | collective-permute-start | bytes 1966088 | tf_op jit(solution)/shard_map/ppermute | solution.py:367
  133.6 13.4 %collective-permute-start.4 = (bf16[64,1024]{1,0:T(8,128)(2,1)}, bf16[64,1024]{1,0:T(8,128)(2,1)}, u32[]{:S(2)}, u32[]{:S(2)}) collective-permute-start(bf16[64,1024]{1,0:T(8,128)(2,1)} %get-tuple-element.35), channel_id=1, source_target_pairs={{0,2},{1,3},{2,0},{3,1},{4,6},{5,7},{6,4},{7,5},{8,10},{9,11},{10,... | collective-permute-start | bytes 393224 | tf_op jit(solution)/shard_map/ppermute | solution.py:367
  143.9 13.8 %collective-permute-start.47 = (bf16[256,512]{1,0:T(8,128)(2,1)}, bf16[256,512]{1,0:T(8,128)(2,1)}, u32[]{:S(2)}, u32[]{:S(2)}) collective-permute-start(bf16[256,512]{1,0:T(8,128)(2,1)} %get-tuple-element.30), channel_id=1, source_target_pairs={{0,4},{4,0},{8,12},{12,8},{16,20},{20,16},{24,28},{28,24},{1,5},{5... | collective-permute-start | bytes 786440 | tf_op jit(solution)/shard_map/ppermute | solution.py:367
  148.0 22.7 %collective-permute-start.5 = (bf16[128,512]{1,0:T(8,128)(2,1)S(1)}, bf16[128,512]{1,0:T(8,128)(2,1)S(1)}, u32[]{:S(2)}, u32[]{:S(2)}) collective-permute-start(bf16[128,512]{1,0:T(8,128)(2,1)S(1)} %get-tuple-element.34), channel_id=1, source_target_pairs={{0,1},{1,0},{2,3},{3,2},{4,5},{5,4},{6,7},{7,6},{8,9},{9,8},{10,11... | collective-permute-start | bytes 393224 | tf_op jit(solution)/shard_map/ppermute | solution.py:367
  155.6 15.1 %copy-start.3 = (f32[256,512]{1,0:T(8,128)}, f32[256,512]{1,0:T(8,128)S(1)}, u32[]{:S(2)}) copy-start(f32[256,512]{1,0:T(8,128)S(1)} %get-tuple-element.20) | copy-start | bytes 1572868
  155.6 9.2 %collective-permute-start.25 = (bf16[256,512]{1,0:T(8,128)(2,1)S(1)}, bf16[256,512]{1,0:T(8,128)(2,1)S(1)}, u32[]{:S(2)}, u32[]{:S(2)}) collective-permute-start(bf16[256,512]{1,0:T(8,128)(2,1)S(1)} %get-tuple-element.24), channel_id=1, source_target_pairs={{0,4},{4,0},{8,12},{12,8},{16,20},{20,16},{24,28},{28,24},{1,5},{5... | collective-permute-start | bytes 786440 | tf_op jit(solution)/shard_map/ppermute | solution.py:367
  156.0 14.5 %collective-permute-start.46 = (bf16[256,512]{1,0:T(8,128)(2,1)S(1)}, bf16[256,512]{1,0:T(8,128)(2,1)S(1)}, u32[]{:S(2)}, u32[]{:S(2)}) collective-permute-start(bf16[256,512]{1,0:T(8,128)(2,1)S(1)} %copy-done.10), channel_id=1, source_target_pairs={{0,4},{4,0},{8,12},{12,8},{16,20},{20,16},{24,28},{28,24},{1,5},{5... | collective-permute-start | bytes 786440 | tf_op jit(solution)/shard_map/ppermute | solution.py:367
  158.7 11.7 %collective-permute-start.48 = (bf16[256,512]{1,0:T(8,128)(2,1)S(1)}, bf16[256,512]{1,0:T(8,128)(2,1)S(1)}, u32[]{:S(2)}, u32[]{:S(2)}) collective-permute-start(bf16[256,512]{1,0:T(8,128)(2,1)S(1)} %add_convert_fusion.2), channel_id=1, source_target_pairs={{0,8},{4,12},{8,0},{12,4},{16,24},{20,28},{24,16},{28,20},{1,9},{5... | collective-permute-start | bytes 786440 | tf_op jit(solution)/shard_map/ppermute | solution.py:367
  158.8 16.8 %collective-permute-start.24 = (bf16[256,512]{1,0:T(8,128)(2,1)}, bf16[256,512]{1,0:T(8,128)(2,1)S(1)}, u32[]{:S(2)}, u32[]{:S(2)}) collective-permute-start(bf16[256,512]{1,0:T(8,128)(2,1)} %get-tuple-element.22), channel_id=1, source_target_pairs={{0,4},{4,0},{8,12},{12,8},{16,20},{20,16},{24,28},{28,24},{1,5},{5... | collective-permute-start | bytes 786440 | tf_op jit(solution)/shard_map/ppermute | solution.py:367
  164.9 10.7 %collective-permute-start.26 = (bf16[256,512]{1,0:T(8,128)(2,1)S(1)}, bf16[256,512]{1,0:T(8,128)(2,1)S(1)}, u32[]{:S(2)}, u32[]{:S(2)}) collective-permute-start(bf16[256,512]{1,0:T(8,128)(2,1)S(1)} %add_convert_fusion.3), channel_id=1, source_target_pairs={{0,8},{4,12},{8,0},{12,4},{16,24},{20,28},{24,16},{28,20},{1,9},{5... | collective-permute-start | bytes 786440 | tf_op jit(solution)/shard_map/ppermute | solution.py:367
  170.6 12.9 %collective-permute-start.49 = (bf16[256,512]{1,0:T(8,128)(2,1)S(1)}, bf16[256,512]{1,0:T(8,128)(2,1)S(1)}, u32[]{:S(2)}, u32[]{:S(2)}) collective-permute-start(bf16[256,512]{1,0:T(8,128)(2,1)S(1)} %add_convert_fusion.1), channel_id=1, source_target_pairs={{0,16},{4,20},{8,24},{12,28},{16,0},{20,4},{24,8},{28,12},{1,17},{... | collective-permute-start | bytes 786440 | tf_op jit(solution)/shard_map/ppermute | solution.py:367
  (26 other events, 141.4 us)

commit v2 on v1

--- a/solution.py
+++ b/solution.py
@@ -20,8 +20,9 @@
 NORM_EPS = 1e-05
 LANES = 128
 AHEAD = 2
+RING = AHEAD + 1
 DOWN_AHEAD = 4
-UP_VMEM = 36 * 1024 * 1024
+UP_VMEM = 24 * 1024 * 1024
 DOWN_VMEM = 20 * 1024 * 1024
 
 
@@ -214,8 +215,8 @@
     for e in range(exp_dev):
         copies.append(
             (
-                pltpu.make_async_copy(gate_hbm.at[e], weights_ref.at[e, :piece], sems.at[0, e]),
-                pltpu.make_async_copy(up_hbm.at[e], weights_ref.at[e, piece:], sems.at[1, e]),
+                pltpu.make_async_copy(gate_hbm.at[e], weights_ref.at[e % RING, :piece], sems.at[0, e]),
+                pltpu.make_async_copy(up_hbm.at[e], weights_ref.at[e % RING, piece:], sems.at[1, e]),
             )
         )
     for e in range(min(AHEAD, exp_dev)):
@@ -277,7 +278,7 @@
             for copy in copies[e + AHEAD]:
                 copy.start()
         held = slots_ref[e]
-        both = lax.dot_general(held, weights_ref[e], NT, preferred_element_type=jnp.float32)
+        both = lax.dot_general(held, weights_ref[e % RING], NT, preferred_element_type=jnp.float32)
         hidden_ref[e] = silu_product(both[:, :piece], both[:, piece:])
 
 
@@ -394,15 +395,17 @@
 
     attended = attention(queries, keys, values, sink)
     projected = jnp.dot(attended, w_out, preferred_element_type=f32)
-    quarters = projected.reshape(n_tp // 2, 2, rows, D)
     core = tp_idx % 2
     own_y = tp_idx // 2
-    keep = lax.dynamic_index_in_dim(quarters, core, 1, keepdims=False)
-    give = lax.dynamic_index_in_dim(quarters, 1 - core, 1, keepdims=False)
-    chip = keep + core_swap(give.astype(bf16)).astype(f32)
-    away = lax.dynamic_index_in_dim(chip, 1 - own_y, 0, keepdims=False).astype(bf16)
-    home = lax.dynamic_index_in_dim(chip, own_y, 0, keepdims=False)
-    summed = home + y_swap(away).astype(f32)
+
+    def quarter(y, c):
+        return lax.dynamic_slice_in_dim(projected, (2 * y + c) * rows, rows, 0)
+
+    for_away = core_swap(quarter(1 - own_y, 1 - core).astype(bf16))
+    for_home = core_swap(quarter(own_y, 1 - core).astype(bf16))
+    away = (quarter(1 - own_y, core) + for_away.astype(f32)).astype(bf16)
+    there = y_swap(away)
+    summed = quarter(own_y, core) + for_home.astype(f32) + there.astype(f32)
     mixed = (stream.astype(f32) + summed).astype(bf16)
     wide = mixed.astype(f32)
     scale = lax.rsqrt(jnp.mean(wide * wide, axis=-1, keepdims=True) + NORM_EPS)
@@ -423,6 +426,26 @@
         places += [range(base, base + n_tp), range(base + n_tp, base + 2 * n_tp)]
     quads = n_tp
 
+    block = jnp.concatenate([part[:, :D] for part in chunks[1][0][:n_tp]], axis=0)
+    shared = [
+        lax.dot_general(block, w, NT, preferred_element_type=f32) for w in (shared_gate, shared_up)
+    ]
+    order = jnp.arange(n_tp) ^ tp_idx
+    shared = silu_product(*shared).reshape(n_tp, rows, piece)
+    shared = jnp.take(shared, order, axis=0).reshape(tok_dev, piece)
+    shared_y = y_swap(shared)
+    shared = [shared, core_swap(shared), shared_y, core_swap(shared_y)]
+
+    def shared_of(parts):
+        return sum(
+            jnp.dot(
+                part,
+                lax.dynamic_slice_in_dim(shared_down, (tp_idx ^ place) * piece, piece, 0),
+                preferred_element_type=f32,
+            )
+            for place, part in enumerate(parts)
+        )
+
     def columns(a, index, width):
         return lax.dynamic_slice_in_dim(a, index * width, width, 1)
 
@@ -432,8 +455,10 @@
     by_y = jnp.concatenate([near_y, far_y], axis=0)
     here = columns(by_y, core, d_dev)
     there = core_swap(columns(by_y, 1 - core, d_dev))
-    both = jnp.stack([here[:rows], there[:rows], here[rows:], there[rows:]], axis=0)
-    residual = jnp.take(both, jnp.arange(n_tp) ^ tp_idx, axis=0).reshape(tok_dev, d_dev)
+
+    def residual_of(here, there):
+        both = jnp.stack([here[:rows], there[:rows], here[rows:], there[rows:]], axis=0)
+        return jnp.take(both, order, axis=0).reshape(tok_dev, d_dev).astype(f32)
 
     where = jnp.stack([sp_idx * exp_dev, tp_idx]).astype(jnp.int32)
     width = quads * capacity
@@ -469,7 +494,7 @@
             out_specs=[vmem] * len(out_shape),
             out_shape=out_shape,
             scratch_shapes=[
-                pltpu.VMEM((exp_dev, 2 * piece, D), bf16),
+                pltpu.VMEM((RING, 2 * piece, D), bf16),
                 pltpu.VMEM((exp_dev, units * width, D), bf16),
                 pltpu.SemaphoreType.DMA((2, exp_dev)),
             ]
@@ -514,21 +539,25 @@
             name="down_kernel",
         )(where, *map(in_vmem, hiddens), table, *in_hbm(w_down, *more))
 
-    total = residual.astype(f32)
     sums = {}
     for chunk, (operands, places) in enumerate(chunks):
-        hidden, table = up_call(operands, places, chunk == 1)
+        hidden, table = up_call(operands, places, False)
         by_y = y_swap(hidden)
         hiddens = [hidden, core_swap(hidden)]
         hiddens += [by_y, core_swap(by_y)]
-        parts = list(down_call(hiddens, table, chunk == 1))
+        parts = list(down_call(hiddens, table, False))
+        if chunk == 0:
+            parts, shared, ends = lax.optimization_barrier((parts, shared, (here, there)))
+            total = residual_of(*ends) + shared_of(shared)
         if chunk == 1:
-            total += parts.pop(0)
+            from_next, parts[0] = lax.optimization_barrier((from_next, parts[0]))
         for pair in range(chunk_z):
             k = (1 - chunk) * chunk_z + pair
             there = x_swap(parts[pair * nx + 1])
             sums[k] = parts[pair * nx].astype(f32) + there.astype(f32)
-    from_next = z_swap(sums[3].astype(bf16), 1)
+        if chunk == 0:
+            last, total = lax.optimization_barrier((sums[3].astype(bf16), total))
+            from_next = z_swap(last, 1)
     from_far = z_swap((sums[2] + from_next.astype(f32)).astype(bf16), 2)
     total += sums[0] + z_swap(sums[1].astype(bf16), 1).astype(f32)
     return (total + from_far.astype(f32)).astype(bf16)

time: 186 us -> 186 us (level)
  waiting for transfers between devices: 81.8 us -> 72.9 us
  starting transfers between devices: 39.2 us -> 46.7 us
  matrix products: 1.43 us -> 6.11 us
  Pallas kernels: 40.4 us -> 36 us
  other arithmetic: 8.42 us -> 10.4 us
    ppermute x48 -> x52, waiting for transfers between devices: 79.1 us -> 70.3 us  [swap(): return lax.ppermute(a, axis, pairs)]
    ppermute x48 -> x52, starting transfers between devices: 33 us -> 40.5 us  [swap(): return lax.ppermute(a, axis, pairs)]
    dot_general x0 -> x6, matrix products: none -> 4.68 us  [the longest x4 3.74 us: shared_of(): jnp.dot(part, lax.dynamic_slice_in_dim(shared_down, (tp_idx ^ place) * pi...]
    unnamed x80 -> x78, local copies, waits for them, and re-layouts: 6.07 us -> 2.29 us
    pallas_call x2, Pallas kernels: 26.3 us -> 23 us  [up_call(): pl.pallas_call(kernel, in_specs=[smem] + [hbm] * (len(operands) + 2 + len...]
    slice x0 -> x3, local copies, waits for them, and re-layouts: none -> 2.9 us  [local_torus(): part[:, :D]]
  transfers between devices with their start and end apart: 50 -> 54, of which waited for: 19 -> 22; matrix products, arithmetic and copies ran while one was open for 4% -> 11% of each run, Pallas kernels for 22% -> 19%
where the time goes in v2:
time: 186 us
  waiting for transfers between devices  72.9 us (39%)
  starting transfers between devices  46.7 us (25%)
  Pallas kernels  36 us (19%)
  local copies, waits for them, and re-layouts  12.8 us (7%)
  other arithmetic  10.4 us (6%)
  matrix products  6.11 us (3%)
    ppermute x52, waiting for transfers between devices, swap(): return lax.ppermute(a, axis, pairs)  70.3 us
    ppermute x52, starting transfers between devices, swap(): return lax.ppermute(a, axis, pairs)  40.5 us
    pallas_call x2, Pallas kernels, up_call(): pl.pallas_call(kernel, in_specs=[smem] + [hbm] * (len(operands) + 2 + len...  23 us
    pallas_call x2, Pallas kernels, down_call(): pl.pallas_call(kernel, in_specs=[smem] + [vmem] * (quads + 1) + [hbm] * (...  13.1 us
    ppermute x1, starting transfers between devices, with_halo(): before = lax.ppermute(last, axis, up)  4.87 us
    dot_general x4, matrix products, shared_of(): jnp.dot(part, lax.dynamic_slice_in_dim(shared_down, (tp_idx ^ place) * pi...  3.74 us
  transfers between devices with their start and end apart: 54, of which 22 were waited for; matrix products, arithmetic and copies ran while one was open for 11% of the time, Pallas kernels for 19%

profile of v2, /device:TPU:0, one launch (start us, length us, event | category | flops | bytes accessed | tf_op | source)
XLA Modules:
  0.0 185.8 jit_solution(8614755418850824552)
XLA Ops:
  0.0 1.1 constant_dynamic-slice_fusion.4
  1.2 4.9 %collective-permute-start = (bf16[128,128]{1,0:T(8,128)(2,1)S(1)}, bf16[128,128]{1,0:T(8,128)(2,1)S(1)}, u32[]{:S(2)}, u32[]{:S(2)}) collective-permute-start(bf16[128,128]{1,0:T(8,128)(2,1)S(1)} %get-tuple-element.72), channel_id=1, source_target_pairs={{0,4},{4,8},{8,12},{12,16},{16,20},{20,24},{24,28},{1,5},{5,9},{9,... | collective-permute-start | bytes 98312 | tf_op jit(solution)/shard_map/ppermute | solution.py:36
  6.1 1.3 collective-permute-start.1
  8.1 1.1 reshape.187
  9.2 2.6 %collective-permute-done.1 = bf16[128,128]{1,0:T(8,128)(2,1)S(1)} collective-permute-done((bf16[128,128]{1,0:T(8,128)(2,1)S(1)}, bf16[128,128]{1,0:T(8,128)(2,1)S(1)}, u32[]{:S(2)}, u32[]{:S(2)}) %collective-permute-start.1) | collective-permute-done | bytes 32800 | tf_op jit(solution)/shard_map/ppermute | solution.py:37
  14.3 0.8 dynamic-slice_convert_fusion.1
  16.0 1.0 collective-permute-done.3
  17.0 1.7 add_convert_fusion.5
  18.7 1.5 collective-permute-start.4
  20.5 6.9 %collective-permute-done.4 = bf16[64,2048]{1,0:T(8,128)(2,1)} collective-permute-done((bf16[64,2048]{1,0:T(8,128)(2,1)}, bf16[64,2048]{1,0:T(8,128)(2,1)}, u32[]{:S(2)}, u32[]{:S(2)}) %collective-permute-start.4) | collective-permute-done | bytes 262176 | tf_op jit(solution)/shard_map/ppermute | solution.py:368
  27.3 1.4 fusion.6
  29.0 2.7 %collective-permute-start.5 = (bf16[64,2176]{1,0:T(8,128)(2,1)S(1)}, bf16[64,2176]{1,0:T(8,128)(2,1)S(1)}, u32[]{:S(2)}, u32[]{:S(2)}) collective-permute-start(bf16[64,2176]{1,0:T(8,128)(2,1)S(1)} %concatenate.29.refs_0_), channel_id=1, source_target_pairs={{0,16},{4,20},{8,24},{12,28},{16,0},{20,4},{24,8},{28,12},{1,17},{... | collective-permute-start | bytes 835592 | tf_op jit(solution)/shard_map/ppermute | solution.py:368
  31.6 1.5 collective-permute-start.25
  33.2 2.4 %collective-permute-start.34 = (bf16[64,2176]{1,0:T(8,128)(2,1)S(1)}, bf16[64,2176]{1,0:T(8,128)(2,1)S(1)}, u32[]{:S(2)}, u32[]{:S(2)}) collective-permute-start(bf16[64,2176]{1,0:T(8,128)(2,1)S(1)} %concatenate.29.refs_0_), channel_id=1, source_target_pairs={{0,4},{4,0},{8,12},{12,8},{16,20},{20,16},{24,28},{28,24},{1,5},{5... | collective-permute-start | bytes 835592 | tf_op jit(solution)/shard_map/ppermute | solution.py:368
  35.6 8.2 %collective-permute-done.5.refs_0_ = bf16[64,2176]{1,0:T(8,128)(2,1)S(1)} collective-permute-done((bf16[64,2176]{1,0:T(8,128)(2,1)S(1)}, bf16[64,2176]{1,0:T(8,128)(2,1)S(1)}, u32[]{:S(2)}, u32[]{:S(2)}) %collective-permute-start.5) | collective-permute-done | bytes 278560 | tf_op jit(solution)/shard_map/ppermute | solution.py:368
  43.9 1.6 collective-permute-start.7
  45.5 2.5 %collective-permute-start.9 = (bf16[64,2176]{1,0:T(8,128)(2,1)S(1)}, bf16[64,2176]{1,0:T(8,128)(2,1)S(1)}, u32[]{:S(2)}, u32[]{:S(2)}) collective-permute-start(bf16[64,2176]{1,0:T(8,128)(2,1)S(1)} %collective-permute-done.5.refs_0_), channel_id=1, source_target_pairs={{0,4},{4,0},{8,12},{12,8},{16,20},{20,16},{24,28},{28,24},{1,5},{5... | collective-permute-start | bytes 835592 | tf_op jit(solution)/shard_map/ppermute | solution.py:368
  47.9 1.3 collective-permute-done.38.refs_8_
  49.7 3.2 %collective-permute-done.7.refs_2_ = bf16[64,2176]{1,0:T(8,128)(2,1)S(1)} collective-permute-done((bf16[64,2176]{1,0:T(8,128)(2,1)S(1)}, bf16[64,2176]{1,0:T(8,128)(2,1)S(1)}, u32[]{:S(2)}, u32[]{:S(2)}) %collective-permute-start.7) | collective-permute-done | bytes 278560 | tf_op jit(solution)/shard_map/ppermute | solution.py:368
  52.9 2.5 %collective-permute-start.36 = (bf16[64,2176]{1,0:T(8,128)(2,1)S(1)}, bf16[64,2176]{1,0:T(8,128)(2,1)S(1)}, u32[]{:S(2)}, u32[]{:S(2)}) collective-permute-start(bf16[64,2176]{1,0:T(8,128)(2,1)S(1)} %collective-permute-done.25.refs_2_), channel_id=1, source_target_pairs={{0,4},{4,0},{8,12},{12,8},{16,20},{20,16},{24,28},{28,24},{1,5},{5... | collective-permute-start | bytes 835592 | tf_op jit(solution)/shard_map/ppermute | solution.py:368
  55.4 1.1 collective-permute-done.13.refs_8_
  57.4 5.5 %collective-permute-done.36.refs_6_ = bf16[64,2176]{1,0:T(8,128)(2,1)S(1)} collective-permute-done((bf16[64,2176]{1,0:T(8,128)(2,1)S(1)}, bf16[64,2176]{1,0:T(8,128)(2,1)S(1)}, u32[]{:S(2)}, u32[]{:S(2)}) %collective-permute-start.36) | collective-permute-done | bytes 278560 | tf_op jit(solution)/shard_map/ppermute | solution.py:368
  62.9 1.6 collective-permute-start.11
  64.5 1.5 collective-permute-start.15
  66.0 1.9 %collective-permute-done.42.refs_12_ = bf16[64,2176]{1,0:T(8,128)(2,1)S(1)} collective-permute-done((bf16[64,2176]{1,0:T(8,128)(2,1)S(1)}, bf16[64,2176]{1,0:T(8,128)(2,1)S(1)}, u32[]{:S(2)}, u32[]{:S(2)}) %collective-permute-start.42) | collective-permute-done | bytes 278560 | tf_op jit(solution)/shard_map/ppermute | solution.py:368
  67.9 1.7 collective-permute-start.17
  69.6 1.6 collective-permute-start.44
  71.2 1.4 collective-permute-done.11.refs_6_
  72.6 6.0 %collective-permute-done.15.refs_10_ = bf16[64,2176]{1,0:T(8,128)(2,1)} collective-permute-done((bf16[64,2176]{1,0:T(8,128)(2,1)}, bf16[64,2176]{1,0:T(8,128)(2,1)}, u32[]{:S(2)}, u32[]{:S(2)}) %collective-permute-start.15) | collective-permute-done | bytes 278560 | tf_op jit(solution)/shard_map/ppermute | solution.py:368
  78.6 2.1 %collective-permute-start.19 = (bf16[64,2176]{1,0:T(8,128)(2,1)}, bf16[64,2176]{1,0:T(8,128)(2,1)}, u32[]{:S(2)}, u32[]{:S(2)}) collective-permute-start(bf16[64,2176]{1,0:T(8,128)(2,1)} %collective-permute-done.15.refs_10_), channel_id=1, source_target_pairs={{0,4},{4,0},{8,12},{12,8},{16,20},{20,16},{24,28},{28,24},{1,5},{5... | collective-permute-start | bytes 835592 | tf_op jit(solution)/shard_map/ppermute | solution.py:368
  80.7 3.2 %collective-permute-done.44.refs_14_ = bf16[64,2176]{1,0:T(8,128)(2,1)S(1)} collective-permute-done((bf16[64,2176]{1,0:T(8,128)(2,1)S(1)}, bf16[64,2176]{1,0:T(8,128)(2,1)S(1)}, u32[]{:S(2)}, u32[]{:S(2)}) %collective-permute-start.44) | collective-permute-done | bytes 278560 | tf_op jit(solution)/shard_map/ppermute | solution.py:368
  85.2 3.2 %collective-permute-done.19.refs_14_ = bf16[64,2176]{1,0:T(8,128)(2,1)} collective-permute-done((bf16[64,2176]{1,0:T(8,128)(2,1)}, bf16[64,2176]{1,0:T(8,128)(2,1)}, u32[]{:S(2)}, u32[]{:S(2)}) %collective-permute-start.19) | collective-permute-done | bytes 278560 | tf_op jit(solution)/shard_map/ppermute | solution.py:368
  88.4 0.7 copy-done.32
  89.7 11.4 %up_kernel.3 = (bf16[8,128,256]{2,1,0:T(8,128)(2,1)S(1)}, bf16[4,256,256]{2,1,0:T(8,128)(2,1)S(1)}) custom-call(s32[2]{0:T(128)S(1)} %pad_add_fusion.where_ref, bf16[64,2176]{1,0:T(8,128)(2,1)} %copy-done.7, bf16[64,2176]{1,0:T(8,128)(2,1)} %copy-done.9, bf16[64,2176]{1,0:T(8,128)(2,1)} %copy-done.8, bf16[64,2176]{1,0:T(8,128)(2,1)} %copy-done.10, ...), custom_call_target="tpu_custom_call" | custom-call | tf_op jit(solution)/shard_map/up_kernel/pallas_call | solution.py:491
  101.1 1.6 collective-permute-start.47
  102.7 11.6 %up_kernel.2 = (bf16[8,128,256]{2,1,0:T(8,128)(2,1)S(1)}, bf16[4,256,256]{2,1,0:T(8,128)(2,1)S(1)}) custom-call(s32[2]{0:T(128)S(1)} %pad_add_fusion.where_ref, bf16[64,2176]{1,0:T(8,128)(2,1)} %copy-done.16, bf16[64,2176]{1,0:T(8,128)(2,1)} %copy-done.17, bf16[64,2176]{1,0:T(8,128)(2,1)} %copy-done.18, bf16[64,2176]{1,0:T(8,128)(2,1)} %copy-done.22, ...), custom_call_target="tpu_custom_call" | custom-call | tf_op jit(solution)/shard_map/up_kernel/pallas_call | solution.py:491
  115.1 0.8 constant_dynamic-slice_fusion
  115.9 1.5 collective-permute-start.30
  117.4 1.0 slice.78
  118.4 1.0 slice.77
  119.3 1.0 slice.79
  121.5 7.8 %collective-permute-done.22.refs_2_ = bf16[8,128,256]{2,1,0:T(8,128)(2,1)} collective-permute-done((bf16[8,128,256]{2,1,0:T(8,128)(2,1)S(1)}, bf16[8,128,256]{2,1,0:T(8,128)(2,1)}, u32[]{:S(2)}, u32[]{:S(2)}) %collective-permute-start.22) | collective-permute-done | bytes 524320 | tf_op jit(solution)/shard_map/ppermute | solution.py:368
  131.4 1.6 fusion.21
  133.0 3.5 %collective-permute-done.28 = bf16[256,256]{1,0:T(8,128)(2,1)} collective-permute-done((bf16[256,256]{1,0:T(8,128)(2,1)S(1)}, bf16[256,256]{1,0:T(8,128)(2,1)}, u32[]{:S(2)}, u32[]{:S(2)}) %collective-permute-start.28) | collective-permute-done | bytes 131104 | tf_op jit(solution)/shard_map/ppermute | solution.py:368
  137.1 6.5 %down_kernel.3 = (bf16[256,512]{1,0:T(8,128)(2,1)S(1)}, bf16[256,512]{1,0:T(8,128)(2,1)S(1)}, bf16[256,512]{1,0:T(8,128)(2,1)S(1)}, bf16[256,512]{1,0:T(8,128)(2,1)}) custom-call(s32[2]{0:T(128)S(1)} %pad_add_fusion.where_ref, bf16[8,128,256]{2,1,0:T(8,128)(2,1)S(1)} %get-tuple-element.47.refs_0_, bf16[8,128,256]{2,1,0:T(8,128)(2,1)} %collective-permute-done.46.refs_1_, ...), custom_call_target="tpu_custom_call" | custom-call | tf_op jit(solution)/shard_map/down_kernel/pallas_call | solution.py:527
  145.1 1.7 collective-permute-start.50
  146.8 6.6 %down_kernel.2 = (bf16[256,512]{1,0:T(8,128)(2,1)S(1)}, bf16[256,512]{1,0:T(8,128)(2,1)S(1)}, bf16[256,512]{1,0:T(8,128)(2,1)S(1)}, bf16[256,512]{1,0:T(8,128)(2,1)}) custom-call(s32[2]{0:T(128)S(1)} %pad_add_fusion.where_ref, bf16[8,128,256]{2,1,0:T(8,128)(2,1)S(1)} %get-tuple-element.31.refs_0_, bf16[8,128,256]{2,1,0:T(8,128)(2,1)} %collective-permute-done.21.refs_1_, ...), custom_call_target="tpu_custom_call" | custom-call | tf_op jit(solution)/shard_map/down_kernel/pallas_call | solution.py:527
  153.8 0.9 slice_bitcast_fusion.6
  154.7 0.7 pad_maximum_fusion.1
  155.5 1.5 gather_fusion.1
  157.1 1.1 fusion.12
  158.3 1.1 fusion.14
  159.4 1.2 fusion.16
  160.9 1.2 collective-permute-done.32
  162.2 1.0 add_convert_fusion.3
  163.8 1.5 collective-permute-start.49
  165.4 1.0 add_convert_fusion.2
  166.4 2.0 %collective-permute-start.51 = (bf16[256,512]{1,0:T(8,128)(2,1)S(1)}, bf16[256,512]{1,0:T(8,128)(2,1)S(1)}, u32[]{:S(2)}, u32[]{:S(2)}) collective-permute-start(bf16[256,512]{1,0:T(8,128)(2,1)S(1)} %add_convert_fusion.2), channel_id=1, source_target_pairs={{0,8},{4,12},{8,0},{12,4},{16,24},{20,28},{24,16},{28,20},{1,9},{5... | collective-permute-start | bytes 786440 | tf_op jit(solution)/shard_map/ppermute | solution.py:368
  168.4 4.0 %collective-permute-done.33 = bf16[256,512]{1,0:T(8,128)(2,1)S(1)} collective-permute-done((bf16[256,512]{1,0:T(8,128)(2,1)S(1)}, bf16[256,512]{1,0:T(8,128)(2,1)S(1)}, u32[]{:S(2)}, u32[]{:S(2)}) %collective-permute-start.33) | collective-permute-done | bytes 262176 | tf_op jit(solution)/shard_map/ppermute | solution.py:368
  172.6 2.1 %collective-permute-start.53 = (bf16[256,512]{1,0:T(8,128)(2,1)S(1)}, bf16[256,512]{1,0:T(8,128)(2,1)S(1)}, u32[]{:S(2)}, u32[]{:S(2)}) collective-permute-start(bf16[256,512]{1,0:T(8,128)(2,1)S(1)} %add_convert_fusion.1), channel_id=1, source_target_pairs={{0,16},{4,20},{8,24},{12,28},{16,0},{20,4},{24,8},{28,12},{1,17},{... | collective-permute-start | bytes 786440 | tf_op jit(solution)/shard_map/ppermute | solution.py:368
  174.7 1.8 collective-permute-done.49
  176.4 3.0 %collective-permute-done.51 = bf16[256,512]{1,0:T(8,128)(2,1)S(1)} collective-permute-done((bf16[256,512]{1,0:T(8,128)(2,1)S(1)}, bf16[256,512]{1,0:T(8,128)(2,1)S(1)}, u32[]{:S(2)}, u32[]{:S(2)}) %collective-permute-start.51) | collective-permute-done | bytes 262176 | tf_op jit(solution)/shard_map/ppermute | solution.py:368
  179.5 5.5 %collective-permute-done.53 = bf16[256,512]{1,0:T(8,128)(2,1)S(1)} collective-permute-done((bf16[256,512]{1,0:T(8,128)(2,1)S(1)}, bf16[256,512]{1,0:T(8,128)(2,1)S(1)}, u32[]{:S(2)}, u32[]{:S(2)}) %collective-permute-start.53) | collective-permute-done | bytes 262176 | tf_op jit(solution)/shard_map/ppermute | solution.py:368
  184.9 0.9 add_convert_fusion
  (187 shorter events, 15.3 us)
Async XLA Ops:
  1.2 8.0 %collective-permute-start = (bf16[128,128]{1,0:T(8,128)(2,1)S(1)}, bf16[128,128]{1,0:T(8,128)(2,1)S(1)}, u32[]{:S(2)}, u32[]{:S(2)}) collective-permute-start(bf16[128,128]{1,0:T(8,128)(2,1)S(1)} %get-tuple-element.72), channel_id=1, source_target_pairs={{0,4},{4,8},{8,12},{12,16},{16,20},{20,24},{24,28},{1,5},{5,9},{9,... | collective-permute-start | bytes 98312 | tf_op jit(solution)/shard_map/ppermute | solution.py:36
  6.1 5.8 %collective-permute-start.1 = (bf16[128,128]{1,0:T(8,128)(2,1)S(1)}, bf16[128,128]{1,0:T(8,128)(2,1)S(1)}, u32[]{:S(2)}, u32[]{:S(2)}) collective-permute-start(bf16[128,128]{1,0:T(8,128)(2,1)S(1)} %get-tuple-element.73), channel_id=1, source_target_pairs={{4,0},{8,4},{12,8},{16,12},{20,16},{24,20},{28,24},{5,1},{9,5},{13... | collective-permute-start | bytes 98312 | tf_op jit(solution)/shard_map/ppermute | solution.py:37
  15.1 1.9 %collective-permute-start.3 = (bf16[64,2048]{1,0:T(8,128)(2,1)}, bf16[64,2048]{1,0:T(8,128)(2,1)}, u32[]{:S(2)}, u32[]{:S(2)}) collective-permute-start(bf16[64,2048]{1,0:T(8,128)(2,1)} %get-tuple-element.60), channel_id=1, source_target_pairs={{0,1},{1,0},{2,3},{3,2},{4,5},{5,4},{6,7},{7,6},{8,9},{9,8},{10,11... | collective-permute-start | bytes 786440 | tf_op jit(solution)/shard_map/ppermute | solution.py:368
  15.4 5.1 %collective-permute-start.2 = (bf16[64,2048]{1,0:T(8,128)(2,1)S(1)}, bf16[64,2048]{1,0:T(8,128)(2,1)}, u32[]{:S(2)}, u32[]{:S(2)}) collective-permute-start(bf16[64,2048]{1,0:T(8,128)(2,1)S(1)} %get-tuple-element.59), channel_id=1, source_target_pairs={{0,1},{1,0},{2,3},{3,2},{4,5},{5,4},{6,7},{7,6},{8,9},{9,8},{10,11... | collective-permute-start | bytes 786440 | tf_op jit(solution)/shard_map/ppermute | solution.py:368
  18.7 8.7 %collective-permute-start.4 = (bf16[64,2048]{1,0:T(8,128)(2,1)}, bf16[64,2048]{1,0:T(8,128)(2,1)}, u32[]{:S(2)}, u32[]{:S(2)}) collective-permute-start(bf16[64,2048]{1,0:T(8,128)(2,1)} %add_convert_fusion.5), channel_id=1, source_target_pairs={{0,2},{1,3},{2,0},{3,1},{4,6},{5,7},{6,4},{7,5},{8,10},{9,11},{10,... | collective-permute-start | bytes 786440 | tf_op jit(solution)/shard_map/ppermute | solution.py:368
  28.9 60.8 %copy-start.12 = (bf16[64,2048]{1,0:T(8,128)(2,1)}, bf16[64,2048]{1,0:T(8,128)(2,1)S(1)}, u32[]{:S(2)}) copy-start(bf16[64,2048]{1,0:T(8,128)(2,1)S(1)} %fusion.8) | copy-start | bytes 786436
  29.0 60.7 %copy-start.7 = (bf16[64,2176]{1,0:T(8,128)(2,1)}, bf16[64,2176]{1,0:T(8,128)(2,1)S(1)}, u32[]{:S(2)}) copy-start(bf16[64,2176]{1,0:T(8,128)(2,1)S(1)} %concatenate.29.refs_0_) | copy-start | bytes 835588
  29.0 14.9 %collective-permute-start.5 = (bf16[64,2176]{1,0:T(8,128)(2,1)S(1)}, bf16[64,2176]{1,0:T(8,128)(2,1)S(1)}, u32[]{:S(2)}, u32[]{:S(2)}) collective-permute-start(bf16[64,2176]{1,0:T(8,128)(2,1)S(1)} %concatenate.29.refs_0_), channel_id=1, source_target_pairs={{0,16},{4,20},{8,24},{12,28},{16,0},{20,4},{24,8},{28,12},{1,17},{... | collective-permute-start | bytes 835592 | tf_op jit(solution)/shard_map/ppermute | solution.py:368
  31.6 12.2 %collective-permute-start.25 = (bf16[64,2176]{1,0:T(8,128)(2,1)S(1)}, bf16[64,2176]{1,0:T(8,128)(2,1)S(1)}, u32[]{:S(2)}, u32[]{:S(2)}) collective-permute-start(bf16[64,2176]{1,0:T(8,128)(2,1)S(1)} %concatenate.29.refs_0_), channel_id=1, source_target_pairs={{0,2},{1,3},{2,0},{3,1},{4,6},{5,7},{6,4},{7,5},{8,10},{9,11},{10,... | collective-permute-start | bytes 835592 | tf_op jit(solution)/shard_map/ppermute | solution.py:368
  33.2 12.3 %collective-permute-start.24 = (bf16[64,2176]{1,0:T(8,128)(2,1)S(1)}, bf16[64,2176]{1,0:T(8,128)(2,1)S(1)}, u32[]{:S(2)}, u32[]{:S(2)}) collective-permute-start(bf16[64,2176]{1,0:T(8,128)(2,1)S(1)} %concatenate.29.refs_0_), channel_id=1, source_target_pairs={{0,1},{1,0},{2,3},{3,2},{4,5},{5,4},{6,7},{7,6},{8,9},{9,8},{10,11... | collective-permute-start | bytes 835592 | tf_op jit(solution)/shard_map/ppermute | solution.py:368
  33.2 14.8 %collective-permute-start.34 = (bf16[64,2176]{1,0:T(8,128)(2,1)S(1)}, bf16[64,2176]{1,0:T(8,128)(2,1)S(1)}, u32[]{:S(2)}, u32[]{:S(2)}) collective-permute-start(bf16[64,2176]{1,0:T(8,128)(2,1)S(1)} %concatenate.29.refs_0_), channel_id=1, source_target_pairs={{0,4},{4,0},{8,12},{12,8},{16,20},{20,16},{24,28},{28,24},{1,5},{5... | collective-permute-start | bytes 835592 | tf_op jit(solution)/shard_map/ppermute | solution.py:368
  35.6 13.6 %collective-permute-start.38 = (bf16[64,2176]{1,0:T(8,128)(2,1)S(1)}, bf16[64,2176]{1,0:T(8,128)(2,1)S(1)}, u32[]{:S(2)}, u32[]{:S(2)}) collective-permute-start(bf16[64,2176]{1,0:T(8,128)(2,1)S(1)} %concatenate.29.refs_0_), channel_id=1, source_target_pairs={{0,8},{4,12},{8,0},{12,4},{16,24},{20,28},{24,16},{28,20},{1,9},{5... | collective-permute-start | bytes 835592 | tf_op jit(solution)/shard_map/ppermute | solution.py:368
  43.9 45.8 %copy-start.16 = (bf16[64,2176]{1,0:T(8,128)(2,1)}, bf16[64,2176]{1,0:T(8,128)(2,1)S(1)}, u32[]{:S(2)}) copy-start(bf16[64,2176]{1,0:T(8,128)(2,1)S(1)} %collective-permute-done.5.refs_0_) | copy-start | bytes 835588
  43.9 5.3 %collective-permute-start.6 = (bf16[64,2176]{1,0:T(8,128)(2,1)S(1)}, bf16[64,2176]{1,0:T(8,128)(2,1)S(1)}, u32[]{:S(2)}, u32[]{:S(2)}) collective-permute-start(bf16[64,2176]{1,0:T(8,128)(2,1)S(1)} %collective-permute-done.5.refs_0_), channel_id=1, source_target_pairs={{0,1},{1,0},{2,3},{3,2},{4,5},{5,4},{6,7},{7,6},{8,9},{9,8},{10,11... | collective-permute-start | bytes 835592 | tf_op jit(solution)/shard_map/ppermute | solution.py:368
  43.9 45.8 %copy-start.8 = (bf16[64,2176]{1,0:T(8,128)(2,1)}, bf16[64,2176]{1,0:T(8,128)(2,1)S(1)}, u32[]{:S(2)}) copy-start(bf16[64,2176]{1,0:T(8,128)(2,1)S(1)} %collective-permute-done.25.refs_2_) | copy-start | bytes 835588
  43.9 9.1 %collective-permute-start.7 = (bf16[64,2176]{1,0:T(8,128)(2,1)S(1)}, bf16[64,2176]{1,0:T(8,128)(2,1)S(1)}, u32[]{:S(2)}, u32[]{:S(2)}) collective-permute-start(bf16[64,2176]{1,0:T(8,128)(2,1)S(1)} %collective-permute-done.5.refs_0_), channel_id=1, source_target_pairs={{0,2},{1,3},{2,0},{3,1},{4,6},{5,7},{6,4},{7,5},{8,10},{9,11},{10,... | collective-permute-start | bytes 835592 | tf_op jit(solution)/shard_map/ppermute | solution.py:368
  45.5 44.3 %copy-start.9 = (bf16[64,2176]{1,0:T(8,128)(2,1)}, bf16[64,2176]{1,0:T(8,128)(2,1)S(1)}, u32[]{:S(2)}) copy-start(bf16[64,2176]{1,0:T(8,128)(2,1)S(1)} %collective-permute-done.24.refs_1_) | copy-start | bytes 835588
  45.5 9.9 %collective-permute-start.9 = (bf16[64,2176]{1,0:T(8,128)(2,1)S(1)}, bf16[64,2176]{1,0:T(8,128)(2,1)S(1)}, u32[]{:S(2)}, u32[]{:S(2)}) collective-permute-start(bf16[64,2176]{1,0:T(8,128)(2,1)S(1)} %collective-permute-done.5.refs_0_), channel_id=1, source_target_pairs={{0,4},{4,0},{8,12},{12,8},{16,20},{20,16},{24,28},{28,24},{1,5},{5... | collective-permute-start | bytes 835592 | tf_op jit(solution)/shard_map/ppermute | solution.py:368
  47.9 24.7 %copy-start.20 = (bf16[64,2176]{1,0:T(8,128)(2,1)}, bf16[64,2176]{1,0:T(8,128)(2,1)S(1)}, u32[]{:S(2)}) copy-start(bf16[64,2176]{1,0:T(8,128)(2,1)S(1)} %collective-permute-done.34.refs_4_) | copy-start | bytes 835588
  47.9 8.5 %collective-permute-start.13 = (bf16[64,2176]{1,0:T(8,128)(2,1)S(1)}, bf16[64,2176]{1,0:T(8,128)(2,1)}, u32[]{:S(2)}, u32[]{:S(2)}) collective-permute-start(bf16[64,2176]{1,0:T(8,128)(2,1)S(1)} %collective-permute-done.5.refs_0_), channel_id=1, source_target_pairs={{0,8},{4,12},{8,0},{12,4},{16,24},{20,28},{24,16},{28,20},{1,9},{5... | collective-permute-start | bytes 835592 | tf_op jit(solution)/shard_map/ppermute | solution.py:368
  49.2 23.4 %copy-start.21 = (bf16[64,2176]{1,0:T(8,128)(2,1)}, bf16[64,2176]{1,0:T(8,128)(2,1)S(1)}, u32[]{:S(2)}) copy-start(bf16[64,2176]{1,0:T(8,128)(2,1)S(1)} %collective-permute-done.38.refs_8_) | copy-start | bytes 835588
  49.2 7.8 %collective-permute-start.26 = (bf16[64,2176]{1,0:T(8,128)(2,1)S(1)}, bf16[64,2176]{1,0:T(8,128)(2,1)S(1)}, u32[]{:S(2)}, u32[]{:S(2)}) collective-permute-start(bf16[64,2176]{1,0:T(8,128)(2,1)S(1)} %collective-permute-done.25.refs_2_), channel_id=1, source_target_pairs={{0,1},{1,0},{2,3},{3,2},{4,5},{5,4},{6,7},{7,6},{8,9},{9,8},{10,11... | collective-permute-start | bytes 835592 | tf_op jit(solution)/shard_map/ppermute | solution.py:368
  49.2 40.4 %copy-start.17 = (bf16[64,2176]{1,0:T(8,128)(2,1)}, bf16[64,2176]{1,0:T(8,128)(2,1)S(1)}, u32[]{:S(2)}) copy-start(bf16[64,2176]{1,0:T(8,128)(2,1)S(1)} %collective-permute-done.6.refs_1_) | copy-start | bytes 835588
  49.2 8.1 %collective-permute-start.35 = (bf16[64,2176]{1,0:T(8,128)(2,1)S(1)}, bf16[64,2176]{1,0:T(8,128)(2,1)}, u32[]{:S(2)}, u32[]{:S(2)}) collective-permute-start(bf16[64,2176]{1,0:T(8,128)(2,1)S(1)} %collective-permute-done.34.refs_4_), channel_id=1, source_target_pairs={{0,1},{1,0},{2,3},{3,2},{4,5},{5,4},{6,7},{7,6},{8,9},{9,8},{10,11... | collective-permute-start | bytes 835592 | tf_op jit(solution)/shard_map/ppermute | solution.py:368
  52.9 10.0 %collective-permute-start.36 = (bf16[64,2176]{1,0:T(8,128)(2,1)S(1)}, bf16[64,2176]{1,0:T(8,128)(2,1)S(1)}, u32[]{:S(2)}, u32[]{:S(2)}) collective-permute-start(bf16[64,2176]{1,0:T(8,128)(2,1)S(1)} %collective-permute-done.25.refs_2_), channel_id=1, source_target_pairs={{0,4},{4,0},{8,12},{12,8},{16,20},{20,16},{24,28},{28,24},{1,5},{5... | collective-permute-start | bytes 835592 | tf_op jit(solution)/shard_map/ppermute | solution.py:368
  55.4 7.5 %collective-permute-start.39 = (bf16[64,2176]{1,0:T(8,128)(2,1)S(1)}, bf16[64,2176]{1,0:T(8,128)(2,1)S(1)}, u32[]{:S(2)}, u32[]{:S(2)}) collective-permute-start(bf16[64,2176]{1,0:T(8,128)(2,1)S(1)} %collective-permute-done.38.refs_8_), channel_id=1, source_target_pairs={{0,1},{1,0},{2,3},{3,2},{4,5},{5,4},{6,7},{7,6},{8,9},{9,8},{10,11... | collective-permute-start | bytes 835592 | tf_op jit(solution)/shard_map/ppermute | solution.py:368
  56.5 8.1 %collective-permute-start.40 = (bf16[64,2176]{1,0:T(8,128)(2,1)S(1)}, bf16[64,2176]{1,0:T(8,128)(2,1)S(1)}, u32[]{:S(2)}, u32[]{:S(2)}) collective-permute-start(bf16[64,2176]{1,0:T(8,128)(2,1)S(1)} %collective-permute-done.38.refs_8_), channel_id=1, source_target_pairs={{0,2},{1,3},{2,0},{3,1},{4,6},{5,7},{6,4},{7,5},{8,10},{9,11},{10,... | collective-permute-start | bytes 835592 | tf_op jit(solution)/shard_map/ppermute | solution.py:368
  57.0 32.7 %copy-start.10 = (bf16[64,2176]{1,0:T(8,128)(2,1)}, bf16[64,2176]{1,0:T(8,128)(2,1)S(1)}, u32[]{:S(2)}) copy-start(bf16[64,2176]{1,0:T(8,128)(2,1)S(1)} %collective-permute-done.26.refs_3_) | copy-start | bytes 835588
  57.0 10.9 %collective-permute-start.42 = (bf16[64,2176]{1,0:T(8,128)(2,1)S(1)}, bf16[64,2176]{1,0:T(8,128)(2,1)S(1)}, u32[]{:S(2)}, u32[]{:S(2)}) collective-permute-start(bf16[64,2176]{1,0:T(8,128)(2,1)S(1)} %collective-permute-done.38.refs_8_), channel_id=1, source_target_pairs={{0,4},{4,0},{8,12},{12,8},{16,20},{20,16},{24,28},{28,24},{1,5},{5... | collective-permute-start | bytes 835592 | tf_op jit(solution)/shard_map/ppermute | solution.py:368
  57.4 12.3 %collective-permute-start.8 = (bf16[64,2176]{1,0:T(8,128)(2,1)S(1)}, bf16[64,2176]{1,0:T(8,128)(2,1)S(1)}, u32[]{:S(2)}, u32[]{:S(2)}) collective-permute-start(bf16[64,2176]{1,0:T(8,128)(2,1)S(1)} %collective-permute-done.7.refs_2_), channel_id=1, source_target_pairs={{0,1},{1,0},{2,3},{3,2},{4,5},{5,4},{6,7},{7,6},{8,9},{9,8},{10,11... | collective-permute-start | bytes 835592 | tf_op jit(solution)/shard_map/ppermute | solution.py:368
  62.9 8.3 %collective-permute-start.10 = (bf16[64,2176]{1,0:T(8,128)(2,1)S(1)}, bf16[64,2176]{1,0:T(8,128)(2,1)S(1)}, u32[]{:S(2)}, u32[]{:S(2)}) collective-permute-start(bf16[64,2176]{1,0:T(8,128)(2,1)S(1)} %collective-permute-done.9.refs_4_), channel_id=1, source_target_pairs={{0,1},{1,0},{2,3},{3,2},{4,5},{5,4},{6,7},{7,6},{8,9},{9,8},{10,11... | collective-permute-start | bytes 835592 | tf_op jit(solution)/shard_map/ppermute | solution.py:368
  62.9 21.0 %copy-start.25 = (bf16[64,2176]{1,0:T(8,128)(2,1)}, bf16[64,2176]{1,0:T(8,128)(2,1)S(1)}, u32[]{:S(2)}) copy-start(bf16[64,2176]{1,0:T(8,128)(2,1)S(1)} %collective-permute-done.39.refs_9_) | copy-start | bytes 835588
  62.9 9.7 %collective-permute-start.11 = (bf16[64,2176]{1,0:T(8,128)(2,1)S(1)}, bf16[64,2176]{1,0:T(8,128)(2,1)}, u32[]{:S(2)}, u32[]{:S(2)}) collective-permute-start(bf16[64,2176]{1,0:T(8,128)(2,1)S(1)} %collective-permute-done.9.refs_4_), channel_id=1, source_target_pairs={{0,2},{1,3},{2,0},{3,1},{4,6},{5,7},{6,4},{7,5},{8,10},{9,11},{10,... | collective-permute-start | bytes 835592 | tf_op jit(solution)/shard_map/ppermute | solution.py:368
  64.5 14.1 %collective-permute-start.15 = (bf16[64,2176]{1,0:T(8,128)(2,1)}, bf16[64,2176]{1,0:T(8,128)(2,1)}, u32[]{:S(2)}, u32[]{:S(2)}) collective-permute-start(bf16[64,2176]{1,0:T(8,128)(2,1)} %collective-permute-done.13.refs_8_), channel_id=1, source_target_pairs={{0,2},{1,3},{2,0},{3,1},{4,6},{5,7},{6,4},{7,5},{8,10},{9,11},{10,... | collective-permute-start | bytes 835592 | tf_op jit(solution)/shard_map/ppermute | solution.py:368
  67.9 10.8 %collective-permute-start.17 = (bf16[64,2176]{1,0:T(8,128)(2,1)}, bf16[64,2176]{1,0:T(8,128)(2,1)}, u32[]{:S(2)}, u32[]{:S(2)}) collective-permute-start(bf16[64,2176]{1,0:T(8,128)(2,1)} %collective-permute-done.13.refs_8_), channel_id=1, source_target_pairs={{0,4},{4,0},{8,12},{12,8},{16,20},{20,16},{24,28},{28,24},{1,5},{5... | collective-permute-start | bytes 835592 | tf_op jit(solution)/shard_map/ppermute | solution.py:368
  69.6 14.3 %collective-permute-start.44 = (bf16[64,2176]{1,0:T(8,128)(2,1)S(1)}, bf16[64,2176]{1,0:T(8,128)(2,1)S(1)}, u32[]{:S(2)}, u32[]{:S(2)}) collective-permute-start(bf16[64,2176]{1,0:T(8,128)(2,1)S(1)} %collective-permute-done.42.refs_12_), channel_id=1, source_target_pairs={{0,2},{1,3},{2,0},{3,1},{4,6},{5,7},{6,4},{7,5},{8,10},{9,11},{10,... | collective-permute-start | bytes 835592 | tf_op jit(solution)/shard_map/ppermute | solution.py:368
  71.2 12.7 %collective-permute-start.37 = (bf16[64,2176]{1,0:T(8,128)(2,1)S(1)}, bf16[64,2176]{1,0:T(8,128)(2,1)S(1)}, u32[]{:S(2)}, u32[]{:S(2)}) collective-permute-start(bf16[64,2176]{1,0:T(8,128)(2,1)S(1)} %collective-permute-done.36.refs_6_), channel_id=1, source_target_pairs={{0,1},{1,0},{2,3},{3,2},{4,5},{5,4},{6,7},{7,6},{8,9},{9,8},{10,11... | collective-permute-start | bytes 835592 | tf_op jit(solution)/shard_map/ppermute | solution.py:368
  72.6 11.9 %collective-permute-start.41 = (bf16[64,2176]{1,0:T(8,128)(2,1)S(1)}, bf16[64,2176]{1,0:T(8,128)(2,1)S(1)}, u32[]{:S(2)}, u32[]{:S(2)}) collective-permute-start(bf16[64,2176]{1,0:T(8,128)(2,1)S(1)} %collective-permute-done.40.refs_10_), channel_id=1, source_target_pairs={{0,1},{1,0},{2,3},{3,2},{4,5},{5,4},{6,7},{7,6},{8,9},{9,8},{10,11... | collective-permute-start | bytes 835592 | tf_op jit(solution)/shard_map/ppermute | solution.py:368
  78.6 6.0 %collective-permute-start.43 = (bf16[64,2176]{1,0:T(8,128)(2,1)S(1)}, bf16[64,2176]{1,0:T(8,128)(2,1)S(1)}, u32[]{:S(2)}, u32[]{:S(2)}) collective-permute-start(bf16[64,2176]{1,0:T(8,128)(2,1)S(1)} %collective-permute-done.42.refs_12_), channel_id=1, source_target_pairs={{0,1},{1,0},{2,3},{3,2},{4,5},{5,4},{6,7},{7,6},{8,9},{9,8},{10,11... | collective-permute-start | bytes 835592 | tf_op jit(solution)/shard_map/ppermute | solution.py:368
  78.6 9.7 %collective-permute-start.19 = (bf16[64,2176]{1,0:T(8,128)(2,1)}, bf16[64,2176]{1,0:T(8,128)(2,1)}, u32[]{:S(2)}, u32[]{:S(2)}) collective-permute-start(bf16[64,2176]{1,0:T(8,128)(2,1)} %collective-permute-done.15.refs_10_), channel_id=1, source_target_pairs={{0,4},{4,0},{8,12},{12,8},{16,20},{20,16},{24,28},{28,24},{1,5},{5... | collective-permute-start | bytes 835592 | tf_op jit(solution)/shard_map/ppermute | solution.py:368
  83.9 4.4 %collective-permute-start.45 = (bf16[64,2176]{1,0:T(8,128)(2,1)S(1)}, bf16[64,2176]{1,0:T(8,128)(2,1)S(1)}, u32[]{:S(2)}, u32[]{:S(2)}) collective-permute-start(bf16[64,2176]{1,0:T(8,128)(2,1)S(1)} %collective-permute-done.44.refs_14_), channel_id=1, source_target_pairs={{0,1},{1,0},{2,3},{3,2},{4,5},{5,4},{6,7},{7,6},{8,9},{9,8},{10,11... | collective-permute-start | bytes 835592 | tf_op jit(solution)/shard_map/ppermute | solution.py:368
  84.0 17.2 %collective-permute-start.14 = (bf16[64,2176]{1,0:T(8,128)(2,1)}, bf16[64,2176]{1,0:T(8,128)(2,1)}, u32[]{:S(2)}, u32[]{:S(2)}) collective-permute-start(bf16[64,2176]{1,0:T(8,128)(2,1)} %collective-permute-done.13.refs_8_), channel_id=1, source_target_pairs={{0,1},{1,0},{2,3},{3,2},{4,5},{5,4},{6,7},{7,6},{8,9},{9,8},{10,11... | collective-permute-start | bytes 835592 | tf_op jit(solution)/shard_map/ppermute | solution.py:368
  84.5 18.2 %collective-permute-start.16 = (bf16[64,2176]{1,0:T(8,128)(2,1)}, bf16[64,2176]{1,0:T(8,128)(2,1)}, u32[]{:S(2)}, u32[]{:S(2)}) collective-permute-start(bf16[64,2176]{1,0:T(8,128)(2,1)} %collective-permute-done.15.refs_10_), channel_id=1, source_target_pairs={{0,1},{1,0},{2,3},{3,2},{4,5},{5,4},{6,7},{7,6},{8,9},{9,8},{10,11... | collective-permute-start | bytes 835592 | tf_op jit(solution)/shard_map/ppermute | solution.py:368
  84.6 18.1 %collective-permute-start.12 = (bf16[64,2176]{1,0:T(8,128)(2,1)}, bf16[64,2176]{1,0:T(8,128)(2,1)}, u32[]{:S(2)}, u32[]{:S(2)}) collective-permute-start(bf16[64,2176]{1,0:T(8,128)(2,1)} %collective-permute-done.11.refs_6_), channel_id=1, source_target_pairs={{0,1},{1,0},{2,3},{3,2},{4,5},{5,4},{6,7},{7,6},{8,9},{9,8},{10,11... | collective-permute-start | bytes 835592 | tf_op jit(solution)/shard_map/ppermute | solution.py:368
  88.4 14.4 %collective-permute-start.18 = (bf16[64,2176]{1,0:T(8,128)(2,1)}, bf16[64,2176]{1,0:T(8,128)(2,1)}, u32[]{:S(2)}, u32[]{:S(2)}) collective-permute-start(bf16[64,2176]{1,0:T(8,128)(2,1)} %collective-permute-done.17.refs_12_), channel_id=1, source_target_pairs={{0,1},{1,0},{2,3},{3,2},{4,5},{5,4},{6,7},{7,6},{8,9},{9,8},{10,11... | collective-permute-start | bytes 835592 | tf_op jit(solution)/shard_map/ppermute | solution.py:368
  89.1 13.6 %collective-permute-start.20 = (bf16[64,2176]{1,0:T(8,128)(2,1)}, bf16[64,2176]{1,0:T(8,128)(2,1)}, u32[]{:S(2)}, u32[]{:S(2)}) collective-permute-start(bf16[64,2176]{1,0:T(8,128)(2,1)} %collective-permute-done.19.refs_14_), channel_id=1, source_target_pairs={{0,1},{1,0},{2,3},{3,2},{4,5},{5,4},{6,7},{7,6},{8,9},{9,8},{10,11... | collective-permute-start | bytes 835592 | tf_op jit(solution)/shard_map/ppermute | solution.py:368
  101.1 20.3 %collective-permute-start.47 = (bf16[8,128,256]{2,1,0:T(8,128)(2,1)S(1)}, bf16[8,128,256]{2,1,0:T(8,128)(2,1)}, u32[]{:S(2)}, u32[]{:S(2)}) collective-permute-start(bf16[8,128,256]{2,1,0:T(8,128)(2,1)S(1)} %get-tuple-element.47.refs_0_), channel_id=1, source_target_pairs={{0,2},{1,3},{2,0},{3,1},{4,6},{5,7},{6,4},{7,5},{8,10},{9,11},{10,... | collective-permute-start | bytes 1572872 | tf_op jit(solution)/shard_map/ppermute | solution.py:368
  114.3 15.0 %collective-permute-start.22 = (bf16[8,128,256]{2,1,0:T(8,128)(2,1)S(1)}, bf16[8,128,256]{2,1,0:T(8,128)(2,1)}, u32[]{:S(2)}, u32[]{:S(2)}) collective-permute-start(bf16[8,128,256]{2,1,0:T(8,128)(2,1)S(1)} %get-tuple-element.31.refs_0_), channel_id=1, source_target_pairs={{0,2},{1,3},{2,0},{3,1},{4,6},{5,7},{6,4},{7,5},{8,10},{9,11},{10,... | collective-permute-start | bytes 1572872 | tf_op jit(solution)/shard_map/ppermute | solution.py:368
  115.9 15.0 %collective-permute-start.30 = (bf16[64,1024]{1,0:T(8,128)(2,1)}, bf16[64,1024]{1,0:T(8,128)(2,1)}, u32[]{:S(2)}, u32[]{:S(2)}) collective-permute-start(bf16[64,1024]{1,0:T(8,128)(2,1)} %get-tuple-element.63), channel_id=1, source_target_pairs={{0,2},{1,3},{2,0},{3,1},{4,6},{5,7},{6,4},{7,5},{8,10},{9,11},{10,... | collective-permute-start | bytes 393224 | tf_op jit(solution)/shard_map/ppermute | solution.py:368
  120.8 15.7 %collective-permute-start.46 = (bf16[8,128,256]{2,1,0:T(8,128)(2,1)S(1)}, bf16[8,128,256]{2,1,0:T(8,128)(2,1)}, u32[]{:S(2)}, u32[]{:S(2)}) collective-permute-start(bf16[8,128,256]{2,1,0:T(8,128)(2,1)S(1)} %get-tuple-element.47.refs_0_), channel_id=1, source_target_pairs={{0,1},{1,0},{2,3},{3,2},{4,5},{5,4},{6,7},{7,6},{8,9},{9,8},{10,11... | collective-permute-start | bytes 1572872 | tf_op jit(solution)/shard_map/ppermute | solution.py:368
  120.9 24.2 %collective-permute-start.21 = (bf16[8,128,256]{2,1,0:T(8,128)(2,1)S(1)}, bf16[8,128,256]{2,1,0:T(8,128)(2,1)}, u32[]{:S(2)}, u32[]{:S(2)}) collective-permute-start(bf16[8,128,256]{2,1,0:T(8,128)(2,1)S(1)} %get-tuple-element.31.refs_0_), channel_id=1, source_target_pairs={{0,1},{1,0},{2,3},{3,2},{4,5},{5,4},{6,7},{7,6},{8,9},{9,8},{10,11... | collective-permute-start | bytes 1572872 | tf_op jit(solution)/shard_map/ppermute | solution.py:368
  121.4 15.7 %collective-permute-start.48 = (bf16[8,128,256]{2,1,0:T(8,128)(2,1)}, bf16[8,128,256]{2,1,0:T(8,128)(2,1)}, u32[]{:S(2)}, u32[]{:S(2)}) collective-permute-start(bf16[8,128,256]{2,1,0:T(8,128)(2,1)} %collective-permute-done.47.refs_2_), channel_id=1, source_target_pairs={{0,1},{1,0},{2,3},{3,2},{4,5},{5,4},{6,7},{7,6},{8,9},{9,8},{10,11... | collective-permute-start | bytes 1572872 | tf_op jit(solution)/shard_map/ppermute | solution.py:368
  129.3 17.5 %collective-permute-start.23 = (bf16[8,128,256]{2,1,0:T(8,128)(2,1)}, bf16[8,128,256]{2,1,0:T(8,128)(2,1)}, u32[]{:S(2)}, u32[]{:S(2)}) collective-permute-start(bf16[8,128,256]{2,1,0:T(8,128)(2,1)} %collective-permute-done.22.refs_2_), channel_id=1, source_target_pairs={{0,1},{1,0},{2,3},{3,2},{4,5},{5,4},{6,7},{7,6},{8,9},{9,8},{10,11... | collective-permute-start | bytes 1572872 | tf_op jit(solution)/shard_map/ppermute | solution.py:368
  130.9 5.7 %collective-permute-start.28 = (bf16[256,256]{1,0:T(8,128)(2,1)S(1)}, bf16[256,256]{1,0:T(8,128)(2,1)}, u32[]{:S(2)}, u32[]{:S(2)}) collective-permute-start(bf16[256,256]{1,0:T(8,128)(2,1)S(1)} %bitcast_select_fusion.2), channel_id=1, source_target_pairs={{0,2},{1,3},{2,0},{3,1},{4,6},{5,7},{6,4},{7,5},{8,10},{9,11},{10,... | collective-permute-start | bytes 393224 | tf_op jit(solution)/shard_map/ppermute | solution.py:368
  136.6 16.9 %collective-permute-start.31 = (bf16[128,512]{1,0:T(8,128)(2,1)}, bf16[128,512]{1,0:T(8,128)(2,1)}, u32[]{:S(2)}, u32[]{:S(2)}) collective-permute-start(bf16[128,512]{1,0:T(8,128)(2,1)} %get-tuple-element.61), channel_id=1, source_target_pairs={{0,1},{1,0},{2,3},{3,2},{4,5},{5,4},{6,7},{7,6},{8,9},{9,8},{10,11... | collective-permute-start | bytes 393224 | tf_op jit(solution)/shard_map/ppermute | solution.py:368
  136.6 16.9 %collective-permute-start.27 = (bf16[256,256]{1,0:T(8,128)(2,1)S(1)}, bf16[256,256]{1,0:T(8,128)(2,1)}, u32[]{:S(2)}, u32[]{:S(2)}) collective-permute-start(bf16[256,256]{1,0:T(8,128)(2,1)S(1)} %bitcast_select_fusion.2), channel_id=1, source_target_pairs={{0,1},{1,0},{2,3},{3,2},{4,5},{5,4},{6,7},{7,6},{8,9},{9,8},{10,11... | collective-permute-start | bytes 393224 | tf_op jit(solution)/shard_map/ppermute | solution.py:368
  137.1 16.4 %collective-permute-start.29 = (bf16[256,256]{1,0:T(8,128)(2,1)}, bf16[256,256]{1,0:T(8,128)(2,1)}, u32[]{:S(2)}, u32[]{:S(2)}) collective-permute-start(bf16[256,256]{1,0:T(8,128)(2,1)} %collective-permute-done.28), channel_id=1, source_target_pairs={{0,1},{1,0},{2,3},{3,2},{4,5},{5,4},{6,7},{7,6},{8,9},{9,8},{10,11... | collective-permute-start | bytes 393224 | tf_op jit(solution)/shard_map/ppermute | solution.py:368
  145.1 20.3 %collective-permute-start.50 = (bf16[256,512]{1,0:T(8,128)(2,1)}, bf16[256,512]{1,0:T(8,128)(2,1)}, u32[]{:S(2)}, u32[]{:S(2)}) collective-permute-start(bf16[256,512]{1,0:T(8,128)(2,1)} %get-tuple-element.53), channel_id=1, source_target_pairs={{0,4},{4,0},{8,12},{12,8},{16,20},{20,16},{24,28},{28,24},{1,5},{5... | collective-permute-start | bytes 786440 | tf_op jit(solution)/shard_map/ppermute | solution.py:368
  153.4 8.7 %collective-permute-start.32 = (bf16[256,512]{1,0:T(8,128)(2,1)}, bf16[256,512]{1,0:T(8,128)(2,1)}, u32[]{:S(2)}, u32[]{:S(2)}) collective-permute-start(bf16[256,512]{1,0:T(8,128)(2,1)} %get-tuple-element.38), channel_id=1, source_target_pairs={{0,4},{4,0},{8,12},{12,8},{16,20},{20,16},{24,28},{28,24},{1,5},{5... | collective-permute-start | bytes 786440 | tf_op jit(solution)/shard_map/ppermute | solution.py:368
  163.2 9.2 %collective-permute-start.33 = (bf16[256,512]{1,0:T(8,128)(2,1)S(1)}, bf16[256,512]{1,0:T(8,128)(2,1)S(1)}, u32[]{:S(2)}, u32[]{:S(2)}) collective-permute-start(bf16[256,512]{1,0:T(8,128)(2,1)S(1)} %add_convert_fusion.3), channel_id=1, source_target_pairs={{0,8},{4,12},{8,0},{12,4},{16,24},{20,28},{24,16},{28,20},{1,9},{5... | collective-permute-start | bytes 786440 | tf_op jit(solution)/shard_map/ppermute | solution.py:368
  163.3 9.2 %collective-permute-start.52 = (bf16[256,512]{1,0:T(8,128)(2,1)S(1)}, bf16[256,512]{1,0:T(8,128)(2,1)S(1)}, u32[]{:S(2)}, u32[]{:S(2)}) collective-permute-start(bf16[256,512]{1,0:T(8,128)(2,1)S(1)} %copy-done.6), channel_id=1, source_target_pairs={{0,4},{4,0},{8,12},{12,8},{16,20},{20,16},{24,28},{28,24},{1,5},{5... | collective-permute-start | bytes 786440 | tf_op jit(solution)/shard_map/ppermute | solution.py:368
  163.8 12.6 %collective-permute-start.49 = (bf16[256,512]{1,0:T(8,128)(2,1)S(1)}, bf16[256,512]{1,0:T(8,128)(2,1)S(1)}, u32[]{:S(2)}, u32[]{:S(2)}) collective-permute-start(bf16[256,512]{1,0:T(8,128)(2,1)S(1)} %copy-done.4), channel_id=1, source_target_pairs={{0,4},{4,0},{8,12},{12,8},{16,20},{20,16},{24,28},{28,24},{1,5},{5... | collective-permute-start | bytes 786440 | tf_op jit(solution)/shard_map/ppermute | solution.py:368
  166.4 13.1 %collective-permute-start.51 = (bf16[256,512]{1,0:T(8,128)(2,1)S(1)}, bf16[256,512]{1,0:T(8,128)(2,1)S(1)}, u32[]{:S(2)}, u32[]{:S(2)}) collective-permute-start(bf16[256,512]{1,0:T(8,128)(2,1)S(1)} %add_convert_fusion.2), channel_id=1, source_target_pairs={{0,8},{4,12},{8,0},{12,4},{16,24},{20,28},{24,16},{28,20},{1,9},{5... | collective-permute-start | bytes 786440 | tf_op jit(solution)/shard_map/ppermute | solution.py:368
  172.6 12.3 %collective-permute-start.53 = (bf16[256,512]{1,0:T(8,128)(2,1)S(1)}, bf16[256,512]{1,0:T(8,128)(2,1)S(1)}, u32[]{:S(2)}, u32[]{:S(2)}) collective-permute-start(bf16[256,512]{1,0:T(8,128)(2,1)S(1)} %add_convert_fusion.1), channel_id=1, source_target_pairs={{0,16},{4,20},{8,24},{12,28},{16,0},{20,4},{24,8},{28,12},{1,17},{... | collective-permute-start | bytes 786440 | tf_op jit(solution)/shard_map/ppermute | solution.py:368
  (29 other events, 204.3 us)
